TPU v7x, 512 devices: a whole 4x8x8 slice. The times are simulated.
512 devices in a mesh: sp: 64 (over z, y), fs: 4 (over x), tp: 2 (over core).
Axes of the slice: x: 4, y: 8, z: 8, core: 2. Of those that a mesh axis runs over, the one named last changes fastest.
Arguments:
- tokens: bfloat16 [4, 16384, 1024], P('fs', 'sp', 'tp'), may hold values from -6 to 6
- w_inner: bfloat16 [1024, 2048], P('sp', 'tp'), may hold values from -0.1875 to 0.1875
- w_gate: bfloat16 [1024, 2048], P('sp', 'tp'), may hold values from -0.1875 to 0.1875
- w_write: bfloat16 [1024, 512], P('sp', 'tp'), may hold values from -0.1875 to 0.1875
- w_read: bfloat16 [1024, 512], P('sp', 'tp'), may hold values from -0.1875 to 0.1875
- w_pool_in: bfloat16 [1024, 1024], P('sp', 'tp'), may hold values from -0.1875 to 0.1875
- w_step: bfloat16 [1024, 2, 32], replicated, may hold values from -0.1875 to 0.1875
- conv_inner: bfloat16 [5, 2048], replicated, may hold values from -2.5 to 2.5
- conv_cross: bfloat16 [5, 2, 512], replicated, may hold values from -2.5 to 2.5
- rate_log: float32 [2, 32], replicated, may hold values from -20 to -3
- decay_extra: float32 [4, 16384, 2, 32], P('fs', 'sp', None, 'tp'), may hold values from -1 to 0
- norm_gain: float32 [2048], replicated, may hold values from 0.1 to 1.9
- pool_mix: bfloat16 [4, 256, 256], replicated, may hold values from -0.375 to 0.375
- pool_gain: float32 [1024], replicated, may hold values from 0.1 to 1.9
- w_out_inner: bfloat16 [2048, 1024], P('tp', 'fs'), may hold values from -0.109375 to 0.109375
- w_out_pool: bfloat16 [1024, 1024], P('tp', 'fs'), may hold values from -0.109375 to 0.109375
Outputs:
- layer_out: bfloat16 [4, 16384, 1024], P('fs', ('sp', 'tp'))
All inputs are finite; a program needn't handle non-finite values.
Results may differ from a plain program's by a relative error of at most 0.0075.
Values may be sent and summed in bfloat16 or wider, within the bound.
A program may use at most 128 MiB of HBM per device.

v0:
```python
import jax
import jax.numpy as jnp
from jax import lax
from jax.sharding import Mesh
from jax.sharding import PartitionSpec as P

HEAD_DIM = 64
STATE = 128
POOL_DIM = 256
POOL_GROUPS = 4
CONV = 5
BLOCK = 128
GRID_W = 32
SP = ("sp_0", "sp_1")
SP_TP = ("sp_0", "sp_1", "tp")


EPSILON = 1e-05


def with_halo(block, sides, width):
    for axis, dim in sides:
        count = lax.axis_size(axis)
        forward = [(i, i + 1) for i in range(count - 1)]
        backward = [(target, source) for source, target in forward]
        low = lax.ppermute(
            lax.slice_in_dim(block, block.shape[dim] - width, None, axis=dim), axis, forward
        )
        high = lax.ppermute(lax.slice_in_dim(block, 0, width, axis=dim), axis, backward)
        block = jnp.concatenate([low, block, high], axis=dim)
    return block


def sent_together(arrays, axis, dim, along):
    ends, at = ([], 0)
    for a in arrays[:-1]:
        at += a.shape[along]
        ends.append(at)
    both = jnp.concatenate(arrays, axis=along)
    return tuple(jnp.split(lax.all_gather(both, axis, axis=dim, tiled=True), ends, axis=along))


def sent_to_all(value, axis):
    devices = lax.axis_size(axis)
    return lax.all_to_all(
        jnp.broadcast_to(value[None], (devices, *value.shape)), axis, 0, 0, tiled=True
    )


def in_order(pieces, dim):
    pieces = jnp.moveaxis(pieces, 0, dim)
    lengths = pieces.shape
    return pieces.reshape(*lengths[:dim], lengths[dim] * lengths[dim + 1], *lengths[dim + 2 :])


def gather_directly(value, axis, dim):
    pieces = sent_to_all(value, axis)
    return in_order(pieces, dim)


def nothing_yet(value, identity):
    return jax.tree.map(
        lambda part, zero: jnp.zeros_like(part) + jnp.asarray(zero, part.dtype), value, identity
    )


def prefix_by_axis(value, axes, combine, identity, reverse):
    before = start = nothing_yet(value, identity)
    subtotal = value
    for axis in reversed(axes):
        devices, mine = (lax.axis_size(axis), lax.axis_index(axis))
        pieces = jax.tree.map(
            lambda part, kind: lax.all_gather(part.astype(kind), axis),
            subtotal,
            jax.tree.map(lambda a: jnp.bfloat16 if a.dtype == jnp.float32 else a.dtype, value),
        )
        inside, subtotal = (start, start)
        for k in reversed(range(devices)) if reverse else range(devices):
            passed = k > mine if reverse else k < mine
            subtotal = combine(
                subtotal, jax.tree.map(lambda part, own: part[k].astype(own.dtype), pieces, value)
            )
            inside = jax.tree.map(lambda new, old: jnp.where(passed, new, old), subtotal, inside)
        before = combine(inside, before)
    return before


def cut_along(value, dim, devices):
    before, after = (value.shape[:dim], value.shape[dim + 1 :])
    return jnp.moveaxis(value.reshape(*before, devices, -1, *after), dim, 0)


def sum_at_owner(value, axis, dim):
    pieces = cut_along(value, dim, lax.axis_size(axis))
    arrived = lax.all_to_all(pieces, axis, split_axis=0, concat_axis=0, tiled=True)
    return arrived.astype(jnp.float32).sum(axis=0)


def merge_states(earlier, later):
    return (earlier[0] + later[0], earlier[1] * jnp.exp(later[0])[:, None, None] + later[1])


def local_summary(values, decays, writer_rows, read_rows, per_group):
    tokens_here, heads_here, head_width = values.shape
    groups_here = writer_rows.shape[1]
    blocks = tokens_here // BLOCK
    block_values = values.reshape(blocks, BLOCK, groups_here, per_group, head_width)
    cumulative = jnp.cumsum(
        jnp.transpose(decays.reshape(blocks, BLOCK, heads_here), (0, 2, 1)), axis=2
    )
    cumulative = cumulative.reshape(blocks, groups_here, per_group, BLOCK)
    writes_group = writer_rows.reshape(blocks, BLOCK, groups_here, STATE)
    reads_group = read_rows.reshape(blocks, BLOCK, groups_here, STATE)
    lower_mask = jnp.tril(jnp.ones((BLOCK, BLOCK), dtype=bool))
    segment_log = cumulative[..., :, None] - cumulative[..., None, :]
    weights = jnp.exp(jnp.where(lower_mask, segment_log, -jnp.inf))
    scores = jnp.einsum("bign,bjgn->bgij", reads_group, writes_group)
    inside = jnp.einsum("bgrij,bjgrp->bigrp", scores[:, :, None] * weights, block_values)
    tail_decay = jnp.exp(cumulative[..., -1:] - cumulative)
    block_states = jnp.einsum("bjgn,bgrj,bjgrp->bgrpn", writes_group, tail_decay, block_values)
    block_decay = cumulative[..., -1]
    block_ends = jnp.cumsum(block_decay, axis=0)
    starts = block_ends - block_decay
    order = jnp.arange(blocks, dtype=jnp.int32)
    earlier_mask = (order[:, None] > order[None, :])[:, :, None, None]
    link_decay = jnp.exp(jnp.where(earlier_mask, starts[:, None] - block_ends[None], -jnp.inf))
    entering = jnp.einsum("bcgr,cgrpn->bgrpn", link_decay, block_states)
    device_decay = block_ends[-1]
    summary = jnp.einsum("cgr,cgrpn->grpn", jnp.exp(device_decay[None] - block_ends), block_states)
    parts = (inside, cumulative, starts, entering, reads_group)
    return (
        parts,
        (device_decay.reshape(heads_here), summary.reshape(heads_here, head_width, STATE)),
    )


def finish(parts, incoming):
    inside, cumulative, starts, entering, reads_group = parts
    blocks, groups_here, per_group, block_len = cumulative.shape
    arriving = incoming[1].reshape(
        groups_here, per_group, incoming[1].shape[1], incoming[1].shape[2]
    )
    entering = entering + jnp.exp(starts)[..., None, None] * arriving[None]
    carried = jnp.einsum("bign,bgrpn->bigrp", reads_group, entering)
    carried = carried * jnp.transpose(jnp.exp(cumulative), (0, 3, 1, 2))[..., None]
    outcome = inside + carried
    return outcome.reshape(blocks * block_len, groups_here * per_group, outcome.shape[4])


def pool_local(pool_in, pool_mix, pool_gain, tp_rank, position, devices):
    reach_rows = 2 ** (POOL_GROUPS - 1)
    tokens_here = pool_in.shape[0]
    channels = pool_in.shape[1]
    groups_here = channels // POOL_DIM
    grid_rows = tokens_here // GRID_W
    all_rows = grid_rows * devices
    framed = with_halo(pool_in, ((SP, 0),), reach_rows * GRID_W)
    framed = framed.astype(jnp.float32).reshape(
        grid_rows + 2 * reach_rows, GRID_W, groups_here, POOL_DIM
    )
    row_running = jnp.cumsum(jnp.pad(framed, ((1, 0), (0, 0), (0, 0), (0, 0))), axis=0)
    row_index = position * grid_rows + jnp.arange(grid_rows, dtype=jnp.int32)
    col_index = jnp.arange(GRID_W, dtype=jnp.int32)
    mix_local = lax.dynamic_slice_in_dim(pool_mix, tp_rank * groups_here, groups_here, 0)
    gain_local = lax.dynamic_slice_in_dim(pool_gain, tp_rank * channels, channels, 0)
    results = []
    for slot_index in range(groups_here):
        group_index = tp_rank * groups_here + slot_index
        window = jnp.left_shift(jnp.int32(2), group_index)
        half_window = window // 2
        row_band = row_running[:, :, slot_index]
        box_sum = lax.dynamic_slice_in_dim(
            row_band, reach_rows - half_window + window, grid_rows, 0
        ) - lax.dynamic_slice_in_dim(row_band, reach_rows - half_window, grid_rows, 0)
        col_running = jnp.cumsum(
            jnp.pad(box_sum, ((0, 0), (reach_rows + 1, reach_rows), (0, 0))), axis=1
        )
        box_sum = lax.dynamic_slice_in_dim(
            col_running, reach_rows - half_window + window, GRID_W, 1
        ) - lax.dynamic_slice_in_dim(col_running, reach_rows - half_window, GRID_W, 1)
        row_counts = (
            jnp.clip(row_index - half_window + window, 0, all_rows)
            - jnp.clip(row_index - half_window, 0, all_rows)
        ).astype(jnp.float32)
        col_counts = (
            jnp.clip(col_index - half_window + window, 0, GRID_W)
            - jnp.clip(col_index - half_window, 0, GRID_W)
        ).astype(jnp.float32)
        average = box_sum / (row_counts[:, None, None] * col_counts[None, :, None])
        own_values = framed[reach_rows : reach_rows + grid_rows, :, slot_index]
        offsets = (average - own_values).astype(jnp.bfloat16).reshape(tokens_here, POOL_DIM)
        mixed_rows = jnp.dot(offsets, mix_local[slot_index], preferred_element_type=jnp.float32)
        gain_part = gain_local[slot_index * POOL_DIM : (slot_index + 1) * POOL_DIM]
        results.append((mixed_rows * gain_part).astype(jnp.bfloat16))
    return jnp.concatenate(results, axis=1)


def body(
    tokens,
    w_inner,
    w_gate,
    w_write,
    w_read,
    w_pool_in,
    w_step,
    conv_inner,
    conv_cross,
    rate_log,
    decay_extra,
    norm_gain,
    pool_mix,
    pool_gain,
    w_out_inner,
    w_out_pool,
):
    tp_rank = lax.axis_index("tp")
    out_weights = sent_together((w_out_inner, w_out_pool), "fs", 1, 0)
    whole_rows = gather_directly(tokens[0], "tp", 1)
    tokens_here = whole_rows.shape[0]
    inner_here = w_inner.shape[1]
    cross_here = w_write.shape[1]
    heads_here = inner_here // HEAD_DIM
    groups_here = cross_here // STATE
    per_group = heads_here // groups_here
    stacked = jnp.concatenate([w_inner, w_write, w_read, w_gate, w_pool_in], axis=1)
    projected = jnp.dot(
        whole_rows,
        lax.all_gather(stacked, SP, axis=0, tiled=True),
        preferred_element_type=jnp.float32,
    )
    projected = projected.astype(jnp.bfloat16)
    stream_cols = inner_here + 2 * cross_here
    streams = projected[:, :stream_cols]
    gate_in = projected[:, stream_cols : stream_cols + inner_here]
    pool_in = projected[:, stream_cols + inner_here :]
    rim_width = CONV // 2
    framed = with_halo(streams, ((SP, 0),), rim_width).astype(jnp.float32)
    conv_taps = jnp.concatenate(
        [
            lax.dynamic_slice_in_dim(conv_inner, tp_rank * inner_here, inner_here, 1),
            lax.dynamic_slice_in_dim(conv_cross[:, 0], tp_rank * cross_here, cross_here, 1),
            lax.dynamic_slice_in_dim(conv_cross[:, 1], tp_rank * cross_here, cross_here, 1),
        ],
        axis=1,
    ).astype(jnp.float32)
    running = jnp.zeros((tokens_here, stream_cols), jnp.float32)
    for offset in range(CONV):
        running = running + framed[offset : offset + tokens_here] * conv_taps[offset]
    activated = jax.nn.silu(running)
    values = activated[:, :inner_here].reshape(tokens_here, heads_here, HEAD_DIM)
    writer_rows = activated[:, inner_here : inner_here + cross_here].reshape(
        tokens_here, groups_here, STATE
    )
    read_rows = activated[:, inner_here + cross_here :].reshape(tokens_here, groups_here, STATE)
    step_weights = lax.dynamic_slice_in_dim(w_step, tp_rank * heads_here, heads_here, 2)
    raw_step = jnp.dot(
        whole_rows,
        step_weights.reshape(step_weights.shape[0], 2 * heads_here),
        preferred_element_type=jnp.float32,
    ).reshape(tokens_here, 2, heads_here)
    step_size = jax.nn.softplus(raw_step)
    decay_rates = jnp.exp(lax.dynamic_slice_in_dim(rate_log, tp_rank * heads_here, heads_here, 1))
    log_decay = -step_size * decay_rates[None] + decay_extra[0]
    ahead_parts, ahead_summary = local_summary(
        values * step_size[:, 0, :, None], log_decay[:, 0], writer_rows, read_rows, per_group
    )
    behind_parts, behind_summary = local_summary(
        (values * step_size[:, 1, :, None])[::-1],
        log_decay[::-1, 1],
        writer_rows[::-1],
        read_rows[::-1],
        per_group,
    )
    blank_state = (jnp.zeros_like(ahead_summary[0]), jnp.zeros_like(ahead_summary[1]))
    ahead_in = prefix_by_axis(ahead_summary, SP, merge_states, blank_state, False)
    behind_in = prefix_by_axis(behind_summary, SP, merge_states, blank_state, True)
    pooled = pool_local(
        pool_in, pool_mix, pool_gain, tp_rank, lax.axis_index(SP), lax.axis_size(SP)
    )
    mixed_sum = finish(ahead_parts, ahead_in) + finish(behind_parts, behind_in)[::-1]
    gated_out = mixed_sum * jax.nn.silu(gate_in.astype(jnp.float32)).reshape(
        tokens_here, heads_here, HEAD_DIM
    )
    rms_scale = lax.rsqrt(jnp.mean(gated_out * gated_out, axis=2, keepdims=True) + EPSILON)
    gain_local = lax.dynamic_slice_in_dim(norm_gain, tp_rank * inner_here, inner_here, 0).reshape(
        heads_here, HEAD_DIM
    )
    mixer_out = (
        (gated_out * rms_scale * gain_local).reshape(tokens_here, inner_here).astype(jnp.bfloat16)
    )
    inner_weights, pool_weights = out_weights
    summed = sum_at_owner(
        (
            jnp.dot(mixer_out, inner_weights, preferred_element_type=jnp.float32)
            + jnp.dot(pooled, pool_weights, preferred_element_type=jnp.float32)
        ).astype(jnp.bfloat16),
        "tp",
        0,
    )
    return summed.astype(jnp.bfloat16)[None]


def solution(mesh):
    finer = Mesh(
        mesh.devices.reshape(8, 8, mesh.shape["fs"], mesh.shape["tp"]), ("sp_0", "sp_1", "fs", "tp")
    )
    in_specs = (
        P("fs", SP, "tp"),
        P(SP, "tp"),
        P(SP, "tp"),
        P(SP, "tp"),
        P(SP, "tp"),
        P(SP, "tp"),
        P(),
        P(),
        P(),
        P(),
        P("fs", SP, None, "tp"),
        P(),
        P(),
        P(),
        P("tp", "fs"),
        P("tp", "fs"),
    )
    out_specs = P("fs", SP_TP, None)
    return jax.shard_map(body, mesh=finer, in_specs=in_specs, out_specs=out_specs, check_vma=False)
```

profile of v0, /device:TPU:1, one launch (start us, length us, event | category | flops | bytes accessed | tf_op | source)
XLA Modules:
  0.0 369.2 jit_solution(7352323665303950627)
XLA Ops:
  12.9 10.3 %all-to-all-start = ((bf16[2,256,512]{1,2,0:T(8,128)(2,1)}), bf16[2,256,512]{1,2,0:T(8,128)(2,1)S(1)}, u32[]{:S(2)}, u32[]{:S(2)}) async-start(bf16[2,256,512]{1,2,0:T(8,128)(2,1)} %broadcast_in_dim.44), calls=%async_computation | async-start | bytes 1048576 | tf_op jit(solution)/shard_map/all_to_all | solution.py:45
  27.1 78.8 %all-gather.11.cloned.1.call-done = bf16[1024,3072]{1,0:T(8,128)(2,1)} async-done(((bf16[16,3072]{1,0:T(8,128)(2,1)}), bf16[1024,3072]{1,0:T(8,128)(2,1)}) %all-gather.11.cloned.1.call-update) | async-done | bytes 6291472 | tf_op jit(solution)/shard_map/all_gather | solution.py:228
  105.9 4.6 %fusion = bf16[256,3072]{1,0:T(8,128)(2,1)S(1)} fusion(bf16[1024,3072]{1,0:T(8,128)(2,1)} %all-gather.11.cloned.1.call-done, bf16[256,1024]{0,1:T(8,128)(2,1)S(1)} %bitcast.451), kind=kOutput, calls=%fused_computation.1 | convolution fusion | flops 1611399168 | bytes 8388608 | tf_op jit(solution)/shard_map/dot_general | solution.py:226
  111.9 4.0 %collective-permute-start = (bf16[2,1536]{1,0:T(2,128)(2,1)S(1)}, bf16[2,1536]{1,0:T(2,128)(2,1)S(1)}, u32[]{:S(2)}, u32[]{:S(2)}) collective-permute-start(bf16[2,1536]{1,0:T(2,128)(2,1)S(1)} %get-tuple-element.94), channel_id=1, source_target_pairs={{0,8},{8,16},{16,24},{24,32},{32,40},{40,48},{48,56},{56,64},{64,7... | collective-permute-start | bytes 18440 | tf_op jit(solution)/shard_map/ppermute | solution.py:26
  130.5 14.0 %all-gather = bf16[8,1,16]{2,1,0:T(2,128)(2,1)S(1)} all-gather(bf16[1,1,16]{2,1,0:T(2,128)(2,1)S(1)} %reshape.1178), channel_id=1, replica_groups=mesh['sp_0'=8,'sp_1'=8,'fs'=4,'tp'=2] {'sp_1'}, dimensions={0}, use_global_device_ids=true | all-gather | bytes 288 | tf_op jit(solution)/shard_map/all_gather | solution.py:73
  144.6 19.8 %all-gather.13.cloned.1.call-done = bf16[8,16,64,128]{3,2,1,0:T(8,128)(2,1)} async-done(((bf16[1,16,64,128]{3,2,1,0:T(8,128)(2,1)}), bf16[8,16,64,128]{3,2,1,0:T(8,128)(2,1)}) %all-gather.13.cloned.1.call-update) | async-done | bytes 2097168 | tf_op jit(solution)/shard_map/all_gather | solution.py:73
  164.5 2.7 add_convert_fusion.1
  167.4 11.4 %all-gather.2 = bf16[8,1,16]{2,1,0:T(2,128)(2,1)S(1)} all-gather(bf16[1,1,16]{2,1,0:T(2,128)(2,1)S(1)} %reshape.1182), channel_id=1, replica_groups=mesh['sp_0'=8,'sp_1'=8,'fs'=4,'tp'=2] {'sp_1'}, dimensions={0}, use_global_device_ids=true | all-gather | bytes 288 | tf_op jit(solution)/shard_map/all_gather | solution.py:73
  178.9 29.9 %all-gather.17.cloned.1.call-done = bf16[8,16,64,128]{3,2,1,0:T(8,128)(2,1)} async-done(((bf16[1,16,64,128]{3,2,1,0:T(8,128)(2,1)}), bf16[8,16,64,128]{3,2,1,0:T(8,128)(2,1)}) %all-gather.17.cloned.1.call-update) | async-done | bytes 2097168 | tf_op jit(solution)/shard_map/all_gather | solution.py:73
  208.8 2.7 add_convert_fusion
  221.8 13.7 %all-gather.3 = bf16[8,1,16]{2,1,0:T(2,128)(2,1)S(1)} all-gather(bf16[1,1,16]{2,1,0:T(2,128)(2,1)S(1)} %get-tuple-element.46), channel_id=1, replica_groups=mesh['sp_0'=8,'sp_1'=8,'fs'=4,'tp'=2] {'sp_0'}, dimensions={0}, use_global_device_ids=true | all-gather | bytes 288 | tf_op jit(solution)/shard_map/all_gather | solution.py:73
  235.5 12.3 %all-gather.1 = bf16[8,1,16]{2,1,0:T(2,128)(2,1)S(1)} all-gather(bf16[1,1,16]{2,1,0:T(2,128)(2,1)S(1)} %get-tuple-element.50), channel_id=1, replica_groups=mesh['sp_0'=8,'sp_1'=8,'fs'=4,'tp'=2] {'sp_0'}, dimensions={0}, use_global_device_ids=true | all-gather | bytes 288 | tf_op jit(solution)/shard_map/all_gather | solution.py:73
  272.3 4.7 %collective-permute-start.2 = (bf16[256,512]{1,0:T(8,128)(2,1)S(1)}, bf16[256,512]{1,0:T(8,128)(2,1)}, u32[]{:S(2)}, u32[]{:S(2)}) collective-permute-start(bf16[256,512]{1,0:T(8,128)(2,1)S(1)} %slice.520), channel_id=1, source_target_pairs={{0,8},{8,16},{16,24},{24,32},{32,40},{40,48},{48,56},{56,64},{64,7... | collective-permute-start | bytes 786440 | tf_op jit(solution)/shard_map/ppermute | solution.py:26
  279.6 2.5 maximum_convert_fusion.1
  282.0 2.3 reshape.1139
  287.9 1.9 slice_convert_fusion.15
  290.6 1.9 slice_convert_fusion.7
  292.7 1.8 fusion.242
  301.4 2.1 reshape.1087
  312.4 3.0 reshape.1094
  315.5 2.3 rev.19
  319.7 31.8 %all-gather.21.cloned.1.call-done = bf16[1536,1024]{1,0:T(8,128)(2,1)} async-done(((bf16[1536,256]{1,0:T(8,128)(2,1)}), bf16[1536,1024]{1,0:T(8,128)(2,1)}) %all-gather.21.cloned.1.call-update) | async-done | bytes 3145744 | tf_op jit(solution)/shard_map/all_gather | solution.py:40
  351.5 2.4 fusion.1
  355.7 5.8 %all_to_all.10 = bf16[2,128,1024]{2,1,0:T(8,128)(2,1)S(1)} all-to-all(bf16[2,128,1024]{2,1,0:T(8,128)(2,1)S(1)} %bitcast.452), channel_id=1, replica_groups=mesh['sp_0'=8,'sp_1'=8,'fs'=4,'tp'=2] {'tp'}, dimensions={0} | all-to-all | bytes 1048576 | tf_op jit(solution)/shard_map/all_to_all | solution.py:95
  (381 shorter events, 87.2 us)
Async XLA Ops:
  6.5 280.2 %copy-start = (bf16[4,256,256]{2,1,0:T(8,128)(2,1)S(1)}, bf16[4,256,256]{2,1,0:T(8,128)(2,1)}, u32[]{:S(2)}) copy-start(bf16[4,256,256]{2,1,0:T(8,128)(2,1)} %param.28) | copy-start | bytes 1572868
  6.5 16.7 %copy-start.95 = (f32[2,32]{1,0:T(2,128)S(1)}, f32[2,32]{1,0:T(2,128)}, u32[]{:S(2)}) copy-start(f32[2,32]{1,0:T(2,128)} %param.25) | copy-start | bytes 772
  6.5 16.7 %copy-start.47 = (bf16[1024,2,32]{0,2,1:T(8,128)(2,1)S(1)}, bf16[1024,2,32]{0,2,1:T(8,128)(2,1)}, u32[]{:S(2)}) copy-start(bf16[1024,2,32]{0,2,1:T(8,128)(2,1)} %param.22) | copy-start | bytes 393220
  6.5 99.4 %all-gather.11.cloned.1.call-start = ((), (), s32[]{:S(2)}) async-start(), calls=%async_computation.2 | async-start | bytes 6389760 | tf_op jit(solution)/shard_map/all_gather | solution.py:228
  10.3 14.5 %copy-start.48 = (f32[1,256,2,16]{1,3,2,0:T(8,128)S(1)}, f32[1,256,2,16]{1,3,2,0:T(8,128)}, u32[]{:S(2)}) copy-start(f32[1,256,2,16]{1,3,2,0:T(8,128)} %param.26) | copy-start | bytes 98308
  12.0 14.8 %copy-start.41 = (bf16[5,2,512]{2,1,0:T(2,128)(2,1)S(1)}, bf16[5,2,512]{2,1,0:T(2,128)(2,1)}, u32[]{:S(2)}) copy-start(bf16[5,2,512]{2,1,0:T(2,128)(2,1)} %param.24) | copy-start | bytes 30724
  12.0 15.1 %copy-start.57 = (bf16[5,2048]{1,0:T(8,128)(2,1)S(1)}, bf16[5,2048]{1,0:T(8,128)(2,1)}, u32[]{:S(2)}) copy-start(bf16[5,2048]{1,0:T(8,128)(2,1)} %param.23) | copy-start | bytes 61444
  12.9 11.7 %all-to-all-start = ((bf16[2,256,512]{1,2,0:T(8,128)(2,1)}), bf16[2,256,512]{1,2,0:T(8,128)(2,1)S(1)}, u32[]{:S(2)}, u32[]{:S(2)}) async-start(bf16[2,256,512]{1,2,0:T(8,128)(2,1)} %broadcast_in_dim.44), calls=%async_computation | async-start | bytes 1048576 | tf_op jit(solution)/shard_map/all_to_all | solution.py:45
  23.2 141.3 %all-gather.13.cloned.1.call-start = ((), (), s32[]{:S(2)}) async-start(), calls=%async_computation.3 | async-start | bytes 2359296 | tf_op jit(solution)/shard_map/all_gather | solution.py:73
  26.2 84.4 %copy-start.43 = (f32[2,2,8]{2,1,0:T(2,128)}, f32[2,2,8]{2,1,0:T(2,128)S(1)}, u32[]{:S(2)}) copy-start(f32[2,2,8]{2,1,0:T(2,128)S(1)} %slice_reduce_fusion.1) | copy-start | bytes 388
  26.9 103.5 %copy-start.37 = (f32[2,2,8]{2,1,0:T(2,128)}, f32[2,2,8]{2,1,0:T(2,128)S(1)}, u32[]{:S(2)}) copy-start(f32[2,2,8]{2,1,0:T(2,128)S(1)} %fusion.249) | copy-start | bytes 388
  110.6 5.5 %collective-permute-start.1 = (bf16[2,1536]{1,0:T(2,128)(2,1)S(1)}, bf16[2,1536]{1,0:T(2,128)(2,1)S(1)}, u32[]{:S(2)}, u32[]{:S(2)}) collective-permute-start(bf16[2,1536]{1,0:T(2,128)(2,1)S(1)} %get-tuple-element.95), channel_id=1, source_target_pairs={{8,0},{16,8},{24,16},{32,24},{40,32},{48,40},{56,48},{64,56},{72,6... | collective-permute-start | bytes 18440 | tf_op jit(solution)/shard_map/ppermute | solution.py:29
  111.9 4.8 %collective-permute-start = (bf16[2,1536]{1,0:T(2,128)(2,1)S(1)}, bf16[2,1536]{1,0:T(2,128)(2,1)S(1)}, u32[]{:S(2)}, u32[]{:S(2)}) collective-permute-start(bf16[2,1536]{1,0:T(2,128)(2,1)S(1)} %get-tuple-element.94), channel_id=1, source_target_pairs={{0,8},{8,16},{16,24},{24,32},{32,40},{40,48},{48,56},{56,64},{64,7... | collective-permute-start | bytes 18440 | tf_op jit(solution)/shard_map/ppermute | solution.py:26
  122.3 86.4 %all-gather.17.cloned.1.call-start = ((), (), s32[]{:S(2)}) async-start(), calls=%async_computation.5 | async-start | bytes 2359296 | tf_op jit(solution)/shard_map/all_gather | solution.py:73
  128.9 38.3 %copy-start.22 = (bf16[2,2,8,64,128]{4,3,2,1,0:T(8,128)(2,1)}, bf16[2,2,8,64,128]{4,3,2,1,0:T(8,128)(2,1)S(1)}, u32[]{:S(2)}) copy-start(bf16[2,2,8,64,128]{4,3,2,1,0:T(8,128)(2,1)S(1)} %fusion.43) | copy-start | bytes 1572868
  130.3 36.9 %copy-start.40 = (f32[2,2,8]{2,1,0:T(2,128)S(1)}, f32[2,2,8]{2,1,0:T(2,128)}, u32[]{:S(2)}) copy-start(f32[2,2,8]{2,1,0:T(2,128)} %copy-done.39) | copy-start | bytes 388
  130.4 162.1 %all-gather.15.cloned.1.call-start = ((), (), s32[]{:S(2)}) async-start(), calls=%async_computation.4 | async-start | bytes 2359296 | tf_op jit(solution)/shard_map/all_gather | solution.py:73
  167.2 44.4 %copy-start.20 = (bf16[1024,256]{1,0:T(8,128)(2,1)S(1)}, bf16[1024,256]{1,0:T(8,128)(2,1)}, u32[]{:S(2)}) copy-start(bf16[1024,256]{1,0:T(8,128)(2,1)} %param.30) | copy-start | bytes 1572868
  167.2 44.5 %copy-start.29 = (bf16[512,256]{1,0:T(8,128)(2,1)S(1)}, bf16[512,256]{1,0:T(8,128)(2,1)}, u32[]{:S(2)}) copy-start(bf16[512,256]{1,0:T(8,128)(2,1)} %param.31) | copy-start | bytes 786436
  167.2 136.4 %all-gather.19.cloned.1.call-start = ((), (), s32[]{:S(2)}) async-start(), calls=%async_computation.6 | async-start | bytes 2359296 | tf_op jit(solution)/shard_map/all_gather | solution.py:73
  211.5 55.1 %copy-start.94 = (f32[1024]{0:T(1024)S(1)}, f32[1024]{0:T(1024)}, u32[]{:S(2)}) copy-start(f32[1024]{0:T(1024)} %param.29) | copy-start | bytes 12292
  211.6 139.9 %all-gather.21.cloned.1.call-start = ((), (), s32[]{:S(2)}) async-start(), calls=%async_computation.7 | async-start | bytes 3932160 | tf_op jit(solution)/shard_map/all_gather | solution.py:40
  271.0 8.4 %collective-permute-start.3 = (bf16[256,512]{1,0:T(8,128)(2,1)S(1)}, bf16[256,512]{1,0:T(8,128)(2,1)}, u32[]{:S(2)}, u32[]{:S(2)}) collective-permute-start(bf16[256,512]{1,0:T(8,128)(2,1)S(1)} %slice.520), channel_id=1, source_target_pairs={{8,0},{16,8},{24,16},{32,24},{40,32},{48,40},{56,48},{64,56},{72,6... | collective-permute-start | bytes 786440 | tf_op jit(solution)/shard_map/ppermute | solution.py:29
  272.3 7.3 %collective-permute-start.2 = (bf16[256,512]{1,0:T(8,128)(2,1)S(1)}, bf16[256,512]{1,0:T(8,128)(2,1)}, u32[]{:S(2)}, u32[]{:S(2)}) collective-permute-start(bf16[256,512]{1,0:T(8,128)(2,1)S(1)} %slice.520), channel_id=1, source_target_pairs={{0,8},{8,16},{16,24},{24,32},{32,40},{40,48},{48,56},{56,64},{64,7... | collective-permute-start | bytes 786440 | tf_op jit(solution)/shard_map/ppermute | solution.py:26
  (86 other events, 176.2 us)
Sparse Core Ops, SparseCore 0:
  11.0 94.8 all-gather.10
  122.5 41.9 all-gather.12
  166.5 42.1 all-gather.16
  210.7 42.7 all-gather.14
  255.5 47.0 all-gather.18
  304.5 46.9 all-gather.20
where the time goes:
time: 370 us; the launch traced here: 369 us
  waiting for transfers between devices  163 us (44%)
  local copies, waits for them, and re-layouts  62.2 us (17%)
  blocking collectives  57.1 us (15%)
  other arithmetic  32.1 us (9%)
  starting transfers between devices  21.7 us (6%)
  matrix products  18.1 us (5%)
  between operations  15.2 us (4%)
    all_gather x1, waiting for transfers between devices, body(): lax.all_gather(stacked, SP, axis=0, tiled=True)  78.8 us
    all_gather x4, blocking collectives, prefix_by_axis(): lax.all_gather(part.astype(kind), axis)  51.3 us
    all_gather x4, waiting for transfers between devices, prefix_by_axis(): lax.all_gather(part.astype(kind), axis)  49.8 us
    all_gather x1, waiting for transfers between devices, sent_together(): lax.all_gather(both, axis, axis=dim, tiled=True)  31.8 us
    exp x30, local copies, waits for them, and re-layouts, merge_states(): jnp.exp(later[0])[:, None, None]  19.4 us
    all_to_all x1, starting transfers between devices, sent_to_all(): lax.all_to_all(jnp.broadcast_to(value[None], (devices, *value.shape)), ax...  10.3 us
    ppermute x2, starting transfers between devices, with_halo(): lax.ppermute(lax.slice_in_dim(block, block.shape[dim] - width, None, axis...  8.68 us
    unnamed x205, local copies, waits for them, and re-layouts  7.85 us
  transfers between devices with their start and end apart: 11, of which 7 were waited for; matrix products, arithmetic and copies ran while one was open for 24% of the time, Pallas kernels for 0%

commit v1 on v0

v1 whole, which is shorter than its diff:
```python
import functools

import jax
import jax.numpy as jnp
from jax import lax
from jax.experimental import pallas as pl
from jax.experimental.pallas import tpu as pltpu
from jax.sharding import Mesh
from jax.sharding import PartitionSpec as P

MESH = pl.DeviceIdType.MESH
F32, BF16 = jnp.float32, jnp.bfloat16
HIGHEST = lax.Precision.HIGHEST
SP = ("z", "y")
EPSILON = 1e-05
T = 256
GRID_W = 32


def dot(a, b, dims=((1,), (0,)), **kw):
    return lax.dot_general(a, b, (dims, ((), ())), preferred_element_type=F32, **kw)


def kernel(
    tok, w_inner, w_gate, w_write, w_read, w_pool, wstep, par, rate, dec_in, pmix_in, woi_in, wop_in,
    out,
    x_b, hrow, hall, wa, wb, woi, wop, de, pmix, p_s, hp, y_s, c_s, ea, er, gate, pool, m_s,
    st, dec, r1, d1, r2, d2, res, tot, totd, inc, own, dsend, drecv, xsend, xrecv, mix_s, pld_s,
    lsem, ssem, rsem,
):
    z, y, f, t = (lax.axis_index(a) for a in ("z", "y", "fs", "tp"))
    sp = z * 8 + y
    nxt, prv = lax.rem(sp + 1, 64), lax.rem(sp + 63, 64)
    nxt = {"z": nxt // 8, "y": lax.rem(nxt, 8)}
    prv = {"z": prv // 8, "y": lax.rem(prv, 8)}
    half = f // 2
    counter = [0]
    sent = []

    def send(src, dst, dev):
        i = counter[0]
        counter[0] += 1
        c = pltpu.make_async_remote_copy(
            src_ref=src, dst_ref=dst, send_sem=ssem.at[i], recv_sem=rsem.at[i],
            device_id=dev, device_id_type=MESH,
        )
        c.start()
        sent.append(c)
        return c

    def ymod(d):
        return lax.rem(y + d, 8)

    def zmod(d):
        return lax.rem(z + d, 8)

    def fmod(d):
        return lax.rem(f + d, 4)

    lcount = [0]

    def local(src, dst):
        c = pltpu.make_async_copy(src, dst, lsem.at[lcount[0]])
        lcount[0] += 1
        c.start()
        return c

    peers = [{"y": ymod(d)} for d in range(1, 8)] + [{"z": zmod(d)} for d in range(1, 8)]
    group = [{"fs": fmod(d), "tp": lax.rem(t + e, 2)} for d in range(4) for e in range(2) if d + e]
    peers += group + [nxt, prv]

    own_a, own_b = wa.at[sp], wb.at[sp]
    weights_local = [
        local(w_inner.at[:, pl.ds(pl.multiple_of(f * 256, 256), 256)], own_a.at[:, pl.ds(0, 256)]),
        local(w_write.at[:, pl.ds(pl.multiple_of(half * 128, 128), 128)], own_a.at[:, pl.ds(256, 128)]),
        local(w_read.at[:, pl.ds(pl.multiple_of(half * 128, 128), 128)], own_a.at[:, pl.ds(384, 128)]),
        local(w_gate.at[:, pl.ds(pl.multiple_of(f * 256, 256), 256)], own_b.at[:, pl.ds(0, 256)]),
        local(w_pool.at[:, pl.ds(pl.multiple_of(f * 128, 128), 128)], own_b.at[:, pl.ds(256, 128)]),
    ]
    tok_local = local(tok.at[0], x_b.at[f, t])
    others = [
        local(dec_in.at[f], de.at[f]),
        local(pmix_in.at[t * 2 + half, pl.ds(pl.multiple_of(lax.rem(f, 2) * 128, 128), 128)], pmix),
        local(woi_in.at[pl.ds(pl.multiple_of(f * 256, 256), 256)], woi.at[f]),
        local(wop_in.at[pl.ds(pl.multiple_of(half * 256, 256), 256)], wop.at[f]),
    ]
    barrier = pltpu.get_barrier_semaphore()
    for p in peers:
        pl.semaphore_signal(barrier, inc=1, device_id=p, device_id_type=MESH)
    pl.semaphore_wait(barrier, len(peers))

    tok_local.wait()
    x_own = x_b.at[f, t]
    edge_n = send(x_own.at[pl.ds(240, 16)], hrow.at[0], nxt)
    edge_p = send(x_own.at[pl.ds(0, 16)], hrow.at[1], prv)
    x_right = send(x_own, x_own, {"fs": fmod(1)})
    x_left = send(x_own, x_own, {"fs": fmod(3)})
    x_pair = [send(x_own, x_own, {"tp": 1 - t})]
    for c in weights_local:
        c.wait()
    a1 = [send(own_a, own_a, {"y": ymod(d)}) for d in (1, 7, 2, 6, 3, 5, 4)]
    b1 = [send(own_b, own_b, {"z": zmod(d)}) for d in (1, 7, 2, 6, 3, 5, 4)]

    def slab_a(k):
        return wa.at[pl.ds(pl.multiple_of(zmod(k) * 8, 8), 8)]

    edge_n.wait_recv()
    edge_p.wait_recv()
    local_halo = local(hrow, hall.at[f, t])
    halos = [send(hrow, hall.at[f, t], g) for g in group]
    for c in a1:
        c.wait_recv()
    ar = [send(slab_a(0), slab_a(0), {"z": zmod(1)})]
    al = [send(slab_a(0), slab_a(0), {"z": zmod(7)})]
    for c in b1:
        c.wait_recv()

    def cols_b(k):
        return [wb.at[zz * 8 + ymod(k)] for zz in range(8)]

    br = [[send(s, s, {"y": ymod(1)}) for s in cols_b(0)]]
    bl = [[send(s, s, {"y": ymod(7)}) for s in cols_b(0)]]

    x_right.wait_recv()
    lblk = x_b.at[fmod(3), t]
    x_fr = send(lblk.at[pl.ds(0, 128)], lblk.at[pl.ds(0, 128)], {"fs": fmod(1)})
    x_pair.append(send(lblk, lblk, {"tp": 1 - t}))
    x_left.wait_recv()
    rblk = x_b.at[fmod(1), t]
    x_fl = send(rblk.at[pl.ds(128, 128)], rblk.at[pl.ds(128, 128)], {"fs": fmod(3)})
    x_pair.append(send(rblk, rblk, {"tp": 1 - t}))
    decs = [send(dec_in.at[fmod(d)], de.at[f], {"fs": fmod(d)}) for d in (1, 3, 2)]

    for k in range(1, 4):
        ar[k - 1].wait_recv()
        ar.append(send(slab_a(8 - k), slab_a(8 - k), {"z": zmod(1)}))
        al[k - 1].wait_recv()
        if k < 3:
            al.append(send(slab_a(k), slab_a(k), {"z": zmod(7)}))
        for c in br[k - 1]:
            c.wait_recv()
        br.append([send(s, s, {"y": ymod(1)}) for s in cols_b(8 - k)])
        for c in bl[k - 1]:
            c.wait_recv()
        if k < 3:
            bl.append([send(s, s, {"y": ymod(7)}) for s in cols_b(k)])
        if k == 1:
            x_fr.wait_recv()
            x_fl.wait_recv()
            oblk = x_b.at[fmod(2), t]
            x_pair.append(send(oblk, oblk, {"tp": 1 - t}))
    wos = []
    for d in (1, 3, 2):
        g = fmod(d)
        wos.append(send(woi_in.at[pl.ds(pl.multiple_of(g * 256, 256), 256)], woi.at[f], {"fs": g}))
        wos.append(send(wop_in.at[pl.ds(pl.multiple_of((g // 2) * 256, 256), 256)], wop.at[f], {"fs": g}))
    local_halo.wait()
    for c in others:
        c.wait()
    for c in x_pair + halos + decs:
        c.wait_recv()
    ar[3].wait_recv()
    for c in br[3]:
        c.wait_recv()

    wa0, wa1 = wa[0:32].reshape(512, 512), wa[32:64].reshape(512, 512)
    h0 = hall[:, 0].reshape(128, 512)
    h1 = hall[:, 1].reshape(128, 512)
    hproj = (dot(h0, wa0) + dot(h1, wa1)).astype(BF16).astype(F32)
    side = lax.rem(lax.broadcasted_iota(jnp.int32, (128, 512), 0) // 16, 2)
    gone = jnp.logical_or(
        jnp.logical_and(side == 0, sp == 0), jnp.logical_and(side == 1, sp == 63)
    )
    hp[...] = jnp.where(gone, 0.0, hproj).reshape(4, 2, 16, 512)

    ii = lax.broadcasted_iota(jnp.int32, (T, T), 0)
    jj = lax.broadcasted_iota(jnp.int32, (T, T), 1)
    low = lax.broadcasted_iota(jnp.int32, (T, 128), 1) < 64

    def spread(cols, c):
        parts = [
            jnp.where(low, cols[:, c + 2 * q : c + 2 * q + 1], cols[:, c + 2 * q + 1 : c + 2 * q + 2])
            for q in range(2)
        ]
        return jnp.concatenate(parts, axis=1)

    def front(s, _):
        x0, x1 = x_b[s, 0], x_b[s, 1]
        pa = dot(x0, wa[0:32].reshape(512, 512)) + dot(x1, wa[32:64].reshape(512, 512))
        p_s[16:272, :] = pa.astype(BF16).astype(F32)
        p_s[0:16, :] = hp[s, 0]
        p_s[272:288, :] = hp[s, 1]
        conv = p_s[14 : 14 + T, :] * par[0:1, :]
        for j in range(1, 5):
            conv = conv + p_s[14 + j : 14 + j + T, :] * par[j : j + 1, :]
        act = conv / (1.0 + jnp.exp(-conv))
        v, b, c = act[:, 0:256], act[:, 256:384], act[:, 384:512]
        raw = dot(wstep[:, 0:512], x0, ((1,), (1,))) + dot(wstep[:, 512:1024], x1, ((1,), (1,)))
        step = jnp.maximum(raw, 0.0) + jnp.log1p(jnp.exp(-jnp.abs(raw)))
        ld = de[s] - step * rate[:, 0:1]
        pre = dot(ld, (ii <= jj).astype(F32), precision=HIGHEST)
        suf = dot(ld, (ii >= jj).astype(F32), precision=HIGHEST)
        first = lax.broadcasted_iota(jnp.int32, (8, T), 0) < 4
        cum = jnp.where(first, pre, suf)
        cols = jnp.concatenate([cum, step, jnp.zeros((112, T), F32)], axis=0).T
        bb, cb = b.astype(BF16), c.astype(BF16)
        c_s[s] = cb
        scores = dot(cb, bb, ((1,), (1,)))
        vb = v.astype(BF16)
        ys = []
        for q in range(2):
            vp = vb[:, q * 128 : (q + 1) * 128]
            pair = []
            for e in range(2):
                h = 2 * q + e
                expo = jnp.where(
                    jj <= ii,
                    cols[:, h : h + 1] - cum[h : h + 1, :],
                    cols[:, 4 + h : 5 + h] - cum[4 + h : 5 + h, :],
                )
                df, db = step[h : h + 1, :], step[4 + h : 5 + h, :]
                dts = jnp.where(jj < ii, df, jnp.where(jj > ii, db, df + db))
                pair.append(dot((scores * jnp.exp(expo) * dts).astype(BF16), vp))
            ys.append(jnp.where(low, pair[0], pair[1]))
        y_s[s] = jnp.concatenate(ys, axis=1)
        bt = b.T.astype(BF16)
        ex_a, ex_r = spread(cols, 0), spread(cols, 4)
        end_a, end_r = ex_a[T - 1 : T, :], ex_r[0:1, :]
        vf = (v * (jnp.exp(end_a - ex_a) * spread(cols, 8))).astype(BF16)
        vr = (v * (jnp.exp(end_r - ex_r) * spread(cols, 12))).astype(BF16)
        st[:, 2 * s] = dot(bt, vf).astype(BF16).reshape(8, 16, 256)
        st[:, 2 * s + 1] = dot(bt, vr).astype(BF16).reshape(8, 16, 256)
        dec[2 * s] = jnp.broadcast_to(end_a, (8, 256))
        dec[2 * s + 1] = jnp.broadcast_to(end_r, (8, 256))
        ea[s] = jnp.exp(ex_a)
        er[s] = jnp.exp(ex_r)
        pb = dot(x0, wb[0:32].reshape(512, 384)) + dot(x1, wb[32:64].reshape(512, 384))
        pb = pb.astype(BF16)
        g = pb[:, 0:256].astype(F32)
        gate[s] = g / (1.0 + jnp.exp(-g))
        pool[1, s] = pb[:, 256:384]
        return _

    lax.fori_loop(0, 4, front, 0)

    own_st = local(st.at[y], r1.at[y])
    own_dec = local(dec, d1.at[y])
    s1 = []
    for d in (1, 7, 2, 6, 3, 5, 4):
        s1.append(send(st.at[ymod(d)], r1.at[y], {"y": ymod(d)}))
        s1.append(send(dec, d1.at[y], {"y": ymod(d)}))
    pool_n = send(pool.at[1], pool.at[0], nxt)
    pool_p = send(pool.at[1], pool.at[2], prv)

    g_index = t * 2 + half
    k = jnp.left_shift(jnp.int32(2), g_index)
    ti = lax.broadcasted_iota(jnp.int32, (T, 3 * T), 0)
    tj = lax.broadcasted_iota(jnp.int32, (T, 3 * T), 1)
    ri, ci = ti // GRID_W + 8, ti % GRID_W
    rj, cj = tj // GRID_W, tj % GRID_W
    grow = rj + (sp * 8 - 8)
    inside = (rj >= ri - k // 2) & (rj < ri + k // 2) & (cj >= ci - k // 2) & (cj < ci + k // 2)
    inside = inside & (grow >= 0) & (grow < 512)
    m_s[...] = inside.astype(F32).astype(BF16)

    own_st.wait()
    own_dec.wait()
    for c in s1:
        c.wait_recv()
    for n in range(8):
        run = jnp.zeros((16, 256), F32)
        cumd = jnp.zeros((8, 256), F32)
        for i in range(8) if n % 2 == 0 else reversed(range(8)):
            res[i, n] = run
            tot_d = d1[i, n]
            totd_prev = cumd
            d1[i, n] = totd_prev
            w = jnp.exp(tot_d)
            run = run * jnp.concatenate([w, w], axis=0) + r1[i, n].astype(F32)
            cumd = cumd + tot_d
        tot[n] = run.astype(BF16)
        totd[n] = cumd
    own_t = local(tot, r2.at[z])
    own_td = local(totd, d2.at[z])
    s2 = []
    for d in (1, 7, 2, 6, 3, 5, 4):
        s2.append(send(tot, r2.at[z], {"z": zmod(d)}))
        s2.append(send(totd, d2.at[z], {"z": zmod(d)}))
    own_t.wait()
    own_td.wait()
    for c in s2:
        c.wait_recv()
    for n in range(8):
        acc = jnp.zeros((16, 256), F32)
        for i in range(8) if n % 2 == 0 else reversed(range(8)):
            w = jnp.exp(d2[i, n])
            new = acc * jnp.concatenate([w, w], axis=0) + r2[i, n].astype(F32)
            used = (i < z) if n % 2 == 0 else (i > z)
            acc = jnp.where(used, new, acc)
        for i in range(8):
            w = jnp.exp(d1[i, n])
            r1[i, n] = (res[i, n] + acc * jnp.concatenate([w, w], axis=0)).astype(BF16)
    own_i = local(r1.at[y], inc.at[y])
    s3 = [send(r1.at[ymod(d)], inc.at[y], {"y": ymod(d)}) for d in (1, 7, 2, 6, 3, 5, 4)]

    pool_n.wait_recv()
    pool_p.wait_recv()
    ti1 = lax.broadcasted_iota(jnp.int32, (T, 128), 0)
    row = ti1 // GRID_W + sp * 8
    col = ti1 % GRID_W
    count = (
        (jnp.minimum(row + k // 2, 512) - jnp.maximum(row - k // 2, 0))
        * (jnp.minimum(col + k // 2, GRID_W) - jnp.maximum(col - k // 2, 0))
    ).astype(F32)

    def pools(s, _):
        rows = jnp.concatenate([pool[0, s], pool[1, s], pool[2, s]], axis=0)
        off = dot(m_s[...], rows) / count - pool[1, s].astype(F32)
        mixed = dot(off.astype(BF16), pmix[...]) * par[5:6, 256:512]
        pld_s[s] = mixed.astype(BF16)
        return _

    lax.fori_loop(0, 4, pools, 0)

    own_i.wait()
    for c in s3:
        c.wait_recv()
    for c in wos:
        c.wait_recv()

    blk = (ii // 64 == jj // 64).astype(F32) * (1.0 / 64.0)
    blk = blk.astype(BF16)

    def finish(s):
        cb = c_s[s]
        carried = dot(cb, inc[:, 2 * s].reshape(128, 256)) * ea[s]
        carried = carried + dot(cb, inc[:, 2 * s + 1].reshape(128, 256)) * er[s]
        g = (y_s[s] + carried) * gate[s]
        ms = dot((g * g).astype(BF16), blk)
        mix_s[...] = (g * lax.rsqrt(ms + EPSILON) * par[5:6, 0:256]).astype(BF16)

    pair, far = [], []
    order = [fmod(2), fmod(1), fmod(3), f]
    mine = pl.ds(pl.multiple_of(t * 128, 128), 128)
    theirs = pl.ds(pl.multiple_of((1 - t) * 128, 128), 128)
    for o in range(4):
        s = order[o]
        finish(s)
        for q in range(4):
            cs = slice(q * 256, (q + 1) * 256)
            part = dot(mix_s[theirs, :], woi[q]) + dot(pld_s[s, theirs, :], wop[q])
            dsend[o, :, cs] = part.astype(BF16)
        pair.append((send(dsend.at[o], drecv.at[s], {"tp": 1 - t})))
        for q in range(4):
            cs = slice(q * 256, (q + 1) * 256)
            own[o, :, cs] = dot(mix_s[mine, :], woi[q]) + dot(pld_s[s, mine, :], wop[q])
        pair[o].wait_recv()
        chip = own[o] + drecv[s].astype(F32)
        if o < 3:
            xsend[o] = chip.astype(BF16)
            far.append(send(xsend.at[o], xrecv.at[o], {"fs": s}))
        else:
            own[o] = chip
    for c in far:
        c.wait_recv()
    total = own[3] + xrecv[0].astype(F32) + xrecv[1].astype(F32) + xrecv[2].astype(F32)
    out[0] = total.astype(BF16)
    for c in sent:
        c.wait_send()


N_REMOTE = 160


def body(
    tokens, w_inner, w_gate, w_write, w_read, w_pool_in, w_step, conv_inner, conv_cross, rate_log,
    decay_extra, norm_gain, pool_mix, pool_gain, w_out_inner, w_out_pool,
):
    f, t = lax.axis_index("fs"), lax.axis_index("tp")
    group = t * 2 + f // 2
    h0 = t * 16 + f * 4
    cut = lax.dynamic_slice_in_dim
    wstep = cut(w_step, h0, 4, 2).reshape(1024, 8).T
    taps = jnp.concatenate(
        [
            cut(conv_inner, h0 * 64, 256, 1),
            cut(conv_cross[:, 0], group * 128, 128, 1),
            cut(conv_cross[:, 1], group * 128, 128, 1),
        ],
        axis=1,
    ).astype(F32)
    gains = jnp.concatenate([cut(norm_gain, h0 * 64, 256, 0), cut(pool_gain, group * 256, 256, 0)])
    par = jnp.concatenate([taps, gains[None], jnp.zeros((2, 512), F32)], axis=0)
    rate = jnp.broadcast_to(jnp.exp(cut(rate_log, h0, 4, 1)).reshape(8, 1), (8, 128))
    dec = jnp.transpose(decay_extra[0].reshape(T, 2, 4, 4), (2, 1, 3, 0)).reshape(4, 8, T)
    any_spec = pl.BlockSpec(memory_space=pl.ANY)
    vm = pl.BlockSpec(memory_space=pltpu.VMEM)
    V = pltpu.VMEM
    scratch = [
        V((4, 2, T, 512), BF16),
        V((2, 16, 512), BF16),
        V((4, 2, 2, 16, 512), BF16),
        V((64, 16, 512), BF16),
        V((64, 16, 384), BF16),
        V((4, 256, 256), BF16),
        V((4, 256, 256), BF16),
        V((4, 8, T), F32),
        V((128, 256), BF16),
        V((288, 512), F32),
        V((4, 2, 16, 512), F32),
        V((4, T, 256), F32),
        V((4, T, 128), BF16),
        V((4, T, 256), F32),
        V((4, T, 256), F32),
        V((4, T, 256), F32),
        V((3, 4, T, 128), BF16),
        V((T, 3 * T), BF16),
        V((8, 8, 16, 256), BF16),
        V((8, 8, 256), F32),
        V((8, 8, 16, 256), BF16),
        V((8, 8, 8, 256), F32),
        V((8, 8, 16, 256), BF16),
        V((8, 8, 8, 256), F32),
        V((8, 8, 16, 256), F32),
        V((8, 16, 256), BF16),
        V((8, 8, 256), F32),
        V((8, 8, 16, 256), BF16),
        V((4, 128, 1024), F32),
        V((4, 128, 1024), BF16),
        V((4, 128, 1024), BF16),
        V((3, 128, 1024), BF16),
        V((3, 128, 1024), BF16),
        V((T, 256), BF16),
        V((4, T, 256), BF16),
        pltpu.SemaphoreType.DMA((20,)),
        pltpu.SemaphoreType.DMA((N_REMOTE,)),
        pltpu.SemaphoreType.DMA((N_REMOTE,)),
    ]
    return pl.pallas_call(
        kernel,
        out_shape=jax.ShapeDtypeStruct((1, 128, 1024), BF16),
        in_specs=[any_spec] * 6 + [vm, vm, vm] + [any_spec] * 4,
        out_specs=vm,
        scratch_shapes=scratch,
        compiler_params=pltpu.CompilerParams(
            collective_id=0, has_side_effects=True, vmem_limit_bytes=60 * 1024 * 1024
        ),
    )(
        tokens, w_inner, w_gate, w_write, w_read, w_pool_in, wstep, par, rate, dec, pool_mix,
        w_out_inner, w_out_pool,
    )


def solution(mesh):
    finer = Mesh(
        mesh.devices.reshape(8, 8, mesh.shape["fs"], mesh.shape["tp"]), ("z", "y", "fs", "tp")
    )
    in_specs = (
        P("fs", SP, "tp"),
        P(SP, "tp"),
        P(SP, "tp"),
        P(SP, "tp"),
        P(SP, "tp"),
        P(SP, "tp"),
        P(),
        P(),
        P(),
        P(),
        P("fs", SP, None, "tp"),
        P(),
        P(),
        P(),
        P("tp", "fs"),
        P("tp", "fs"),
    )
    out_specs = P("fs", ("z", "y", "tp"), None)
    return jax.shard_map(body, mesh=finer, in_specs=in_specs, out_specs=out_specs, check_vma=False)
```

time: 370 us -> 132 us (0.36)
  waiting for transfers between devices: 163 us -> 0 us
  Pallas kernels: 0 us -> 124 us
  blocking collectives: 57.1 us -> 0 us
  local copies, waits for them, and re-layouts: 62.2 us -> 6.87 us
  other arithmetic: 32.1 us -> 0.68 us
  starting transfers between devices: 21.7 us -> 0 us
  matrix products: 18.1 us -> 0 us
  between operations: 15.2 us -> 0.08 us
    all_gather x6 -> x0, waiting for transfers between devices: 160 us -> none  [the longest x1 78.8 us: body(): lax.all_gather(stacked, SP, axis=0, tiled=True)]
    pallas_call x0 -> x1, Pallas kernels: none -> 124 us  [body(): pl.pallas_call(kernel, out_shape=jax.ShapeDtypeStruct((1, 128, 1024), BF1...]
    all_gather x4 -> x0, blocking collectives: 51.3 us -> none  [prefix_by_axis(): lax.all_gather(part.astype(kind), axis)]
    exp x37 -> x1, local copies, waits for them, and re-layouts: 21 us -> 0.07 us  [body(): jnp.exp(cut(rate_log, h0, 4, 1)).reshape(8, 1)]
    dot_general x18 -> x0, matrix products: 18.1 us -> none  [the longest x1 4.63 us: body(): jnp.dot(whole_rows, lax.all_gather(stacked, SP, axis=0, tiled=True), pref...]
    convert_element_type x13 -> x1, other arithmetic: 14.2 us -> 0.01 us  [body(): taps = jnp.concatenate([cut(conv_inner, h0 * 64, 256, 1), cut(conv_cross[...]
    ppermute x4 -> x0, starting transfers between devices: 11.3 us -> none  [the longest x2 8.68 us: with_halo(): lax.ppermute(lax.slice_in_dim(block, block.shape[dim] - width, None, axis...]
    all_to_all x1 -> x0, starting transfers between devices: 10.3 us -> none  [sent_to_all(): lax.all_to_all(jnp.broadcast_to(value[None], (devices, *value.shape)), ax...]
  transfers between devices with their start and end apart: 11 -> 0, of which waited for: 7 -> 0; matrix products, arithmetic and copies ran while one was open for 24% -> 0% of each run, Pallas kernels for 0% -> 0%
where the time goes in v1:
time: 132 us; the launch traced here: 131 us
  Pallas kernels  124 us (94%)
  local copies, waits for them, and re-layouts  6.87 us (5%)
    pallas_call x1, Pallas kernels, body(): pl.pallas_call(kernel, out_shape=jax.ShapeDtypeStruct((1, 128, 1024), BF1...  124 us

profile of v1, /device:TPU:1, one launch (start us, length us, event | category | flops | bytes accessed | tf_op | source)
XLA Modules:
  0.0 131.2 jit_solution(7786741420665522191)
XLA Ops:
  0.0 0.0 copy-start
  0.0 0.8 dynamic_slice.32
  0.8 0.0 copy-start.3
  0.8 0.1 pad.2.clone
  0.9 0.6 copy-done.3
  1.5 0.1 fusion
  1.6 0.1 broadcast_in_dim.15
  1.6 0.8 dynamic_slice.31
  2.4 0.7 constant_dynamic-slice_fusion.3
  3.1 0.7 broadcast_in_dim.16.rate
  3.8 0.0 copy-done
  3.8 0.0 copy-start.1
  3.8 0.6 reshape.10
  4.4 0.1 copy-done.1
  4.5 0.0 copy-start.2
  4.6 0.7 maximum_maximum_fusion.par
  5.2 0.1 copy-done.2
  5.3 0.6 reshape.11.dec_in
  5.9 123.6 %shard_map.154 = bf16[1,128,1024]{2,1,0:T(8,128)(2,1)} custom-call(bf16[1,256,512]{2,1,0:T(8,128)(2,1)} %tok.1, bf16[16,1024]{1,0:T(8,128)(2,1)} %w_inner.1, bf16[16,1024]{1,0:T(8,128)(2,1)} %w_gate.1, bf16[16,256]{1,0:T(8,128)(2,1)} %w_write.1, bf16[16,256]{1,0:T(8,128)(2,1)} %w_read.1, bf16[16,512]{1,0:T(8,128)(2,1)} %w_pool.1, bf16[8,1024]{1,0:T(8,128)(2,1)} %bitcast.18, ...), custom_call_target="tpu_custom_call" | custom-call | tf_op jit(solution)/shard_map/pallas_call | solution.py:439
  129.6 1.7 %copy.32 = bf16[1,128,1024]{2,1,0:T(8,128)(2,1)} copy(bf16[1,128,1024]{2,1,0:T(8,128)(2,1)} %shard_map.154) | data formatting | bytes 524288
  (10 shorter events, 0.1 us)
Async XLA Ops:
  0.0 3.8 %copy-start = (bf16[1024,2,32]{0,2,1:T(8,128)(2,1)S(1)}, bf16[1024,2,32]{0,2,1:T(8,128)(2,1)}, u32[]{:S(2)}) copy-start(bf16[1024,2,32]{0,2,1:T(8,128)(2,1)} %param.22) | copy-start | bytes 393220
  0.8 0.7 copy-start.3
  3.8 0.7 copy-start.1
  4.5 0.8 copy-start.2

commit v2 on v1

v2 whole, which is shorter than its diff:
```python
import functools

import jax
import jax.numpy as jnp
from jax import lax
from jax.experimental import pallas as pl
from jax.experimental.pallas import tpu as pltpu
from jax.sharding import Mesh
from jax.sharding import PartitionSpec as P

MESH = pl.DeviceIdType.MESH
F32, BF16 = jnp.float32, jnp.bfloat16
SP = ("z", "y")
EPSILON = 1e-05
T = 256
GRID_W = 32


def silu(v):
    return (0.5 * v) * (1.0 + jnp.tanh(0.5 * v))


def dot(a, b, dims=((1,), (0,)), **kw):
    return lax.dot_general(a, b, (dims, ((), ())), preferred_element_type=F32, **kw)


def kernel(
    tok, w_inner, w_gate, w_write, w_read, w_pool, wst_in, ci_in, cc_in, rate_in, dec_in, ng_in, pmix_in,
    pg_in, woi_in, wop_in,
    out,
    x_b, hrow, hall, wa1, wa2, wb1, wb2, woi, wop, de, pmix, wst, ci, cc, ng, pg, par,
    p_s, hp, y_s, v_s, b_s, c_s, cum_s, stp_s, cols_s, gate, pool, m_s,
    st, dec, r1, d1, pd, r2, d2, totd, res, tot, inc, own, dsend, drecv, raws, rawr, xsend, xrecv,
    mix_s, pld_s,
    lsem, ssem, rsem, psem,
):
    z, y, f, t = (lax.axis_index(a) for a in ("z", "y", "fs", "tp"))
    sp = z * 8 + y
    nxt, prv = lax.rem(sp + 1, 64), lax.rem(sp + 63, 64)
    nxt = {"z": nxt // 8, "y": lax.rem(nxt, 8)}
    prv = {"z": prv // 8, "y": lax.rem(prv, 8)}
    half = f // 2
    group_at = t * 2 + half
    count = [0, 0]
    sent = []

    def send(src, dst, dev):
        i = count[0]
        count[0] += 1
        c = pltpu.make_async_remote_copy(
            src_ref=src, dst_ref=dst, send_sem=ssem.at[i], recv_sem=rsem.at[i],
            device_id=dev, device_id_type=MESH,
        )
        c.start()
        sent.append(c)
        return c

    def local(src, dst):
        c = pltpu.make_async_copy(src, dst, lsem.at[count[1]])
        count[1] += 1
        c.start()
        return c

    def ymod(d):
        return lax.rem(y + d, 8)

    def zmod(d):
        return lax.rem(z + d, 8)

    def fmod(d):
        return lax.rem(f + d, 4)

    def at(v, n):
        return pl.ds(pl.multiple_of(v * n, n), n)

    near_first = (1, 7, 2, 6, 3, 5, 4)
    group = [{"fs": fmod(d), "tp": lax.rem(t + e, 2)} for d in range(4) for e in range(2) if d + e]
    peers = [{"y": ymod(d)} for d in range(1, 8)] + [{"z": zmod(d)} for d in range(1, 8)]
    peers += group + [nxt, prv]
    pair = {"tp": 1 - t}

    pool[0] = jnp.zeros((4, T, 128), BF16)
    pool[2] = jnp.zeros((4, T, 128), BF16)
    barrier = pltpu.get_barrier_semaphore()
    for p in peers:
        pl.semaphore_signal(barrier, inc=1, device_id=p, device_id_type=MESH)
    mine1, mine2, mine3, mine4 = (w.at[z, y] for w in (wa1, wa2, wb1, wb2))
    tok_local = local(tok.at[0], x_b.at[f, t])
    w_local = [
        local(w_inner.at[:, at(f, 256)], mine1),
        local(w_write.at[:, at(half, 128)], mine2.at[:, pl.ds(0, 128)]),
        local(w_read.at[:, at(half, 128)], mine2.at[:, pl.ds(128, 128)]),
        local(w_gate.at[:, at(f, 256)], mine3),
        local(w_pool.at[:, at(f, 128)], mine4),
    ]
    others = [
        local(wst_in.at[:, at(t, 16)], wst),
        local(dec_in.at[:, at(half, 8)], de.at[f]),
        local(ci_in.at[:, at(t * 4 + f, 256)], ci),
        local(cc_in.at[:, :, at(group_at, 128)], cc),
        local(ng_in, ng),
        local(pg_in, pg),
        local(pmix_in.at[group_at, at(lax.rem(f, 2), 128)], pmix),
        local(woi_in.at[at(f, 256)], woi.at[f]),
        local(wop_in.at[at(half, 256)], wop.at[f]),
    ]
    tok_local.wait()
    for c in w_local:
        c.wait()
    pl.semaphore_wait(barrier, len(peers))

    x_own = x_b.at[f, t]
    edge_n = send(x_own.at[pl.ds(240, 16)], hrow.at[0], nxt)
    edge_p = send(x_own.at[pl.ds(0, 16)], hrow.at[1], prv)
    first = [send(mine1, mine1, {"y": ymod(d)}) for d in near_first]
    second = [send(mine2, mine2, {"z": zmod(d)}) for d in near_first]
    x_right = send(x_own, x_own, {"fs": fmod(1)})
    x_left = send(x_own, x_own, {"fs": fmod(3)})
    x_pair = [send(x_own, x_own, pair)]
    decs = [send(dec_in.at[:, at(fmod(d) // 2, 8)], de.at[f], {"fs": fmod(d)}) for d in (1, 3, 2)]
    third = [send(mine3, mine3, {"y": ymod(d)}) for d in near_first]
    fourth = [send(mine4, mine4, {"z": zmod(d)}) for d in near_first]

    def ring_z(w, k, to):
        s = w.at[zmod(8 - k if to == 1 else k)]
        return send(s, s, {"z": zmod(to)})

    def ring_y(w, k, to):
        s = w.at[:, ymod(8 - k if to == 1 else k)]
        return send(s, s, {"y": ymod(to)})

    for c in first:
        c.wait_recv()
    zr, zl = [ring_z(wa1, 0, 1)], [ring_z(wa1, 0, 7)]
    for c in second:
        c.wait_recv()
    yr, yl = [ring_y(wa2, 0, 1)], [ring_y(wa2, 0, 7)]
    edge_n.wait_recv()
    edge_p.wait_recv()
    halo_local = local(hrow, hall.at[f, t])
    halos = [send(hrow, hall.at[f, t], g) for g in group]

    def step(k):
        zr[k - 1].wait_recv()
        zr.append(ring_z(wa1, k, 1))
        zl[k - 1].wait_recv()
        if k < 3:
            zl.append(ring_z(wa1, k, 7))
        yr[k - 1].wait_recv()
        yr.append(ring_y(wa2, k, 1))
        yl[k - 1].wait_recv()
        if k < 3:
            yl.append(ring_y(wa2, k, 7))

    step(1)
    x_right.wait_recv()
    block = x_b.at[fmod(3), t]
    x_fr = send(block.at[pl.ds(0, 128)], block.at[pl.ds(0, 128)], {"fs": fmod(1)})
    x_pair.append(send(block, block, pair))
    x_left.wait_recv()
    block = x_b.at[fmod(1), t]
    x_fl = send(block.at[pl.ds(128, 128)], block.at[pl.ds(128, 128)], {"fs": fmod(3)})
    x_pair.append(send(block, block, pair))
    step(2)
    for c in others:
        c.wait()
    par[0:5, 0:256] = ci[...].astype(F32)
    par[0:5, 256:384] = cc[:, 0, :].astype(F32)
    par[0:5, 384:512] = cc[:, 1, :].astype(F32)
    x_fr.wait_recv()
    x_fl.wait_recv()
    block = x_b.at[fmod(2), t]
    x_pair.append(send(block, block, pair))
    step(3)
    for c in third + fourth:
        c.wait_recv()
    gzr, gzl = [ring_z(wb1, 0, 1)], [ring_z(wb1, 0, 7)]
    gyr, gyl = [ring_y(wb2, 0, 1)], [ring_y(wb2, 0, 7)]

    def gate_step(k):
        for ring, w, make, to in ((gzr, wb1, ring_z, 1), (gyr, wb2, ring_y, 1), (gzl, wb1, ring_z, 7), (gyl, wb2, ring_y, 7)):
            if to == 1 or k < 4:
                ring[k - 1].wait_recv()
            if k < (4 if to == 1 else 3):
                ring.append(make(w, k, to))

    for c in x_pair + decs:
        c.wait_recv()
    ii = lax.broadcasted_iota(jnp.int32, (T, T), 0)
    jj = lax.broadcasted_iota(jnp.int32, (T, T), 1)
    low = lax.broadcasted_iota(jnp.int32, (T, 128), 1) < 64

    def slot_seq(o):
        return lax.rem(f + lax.rem(2 + 3 * o + (3 * o * (o - 1)) // 2, 4), 4)

    r8 = lax.broadcasted_iota(jnp.int32, (8, 1), 0)
    rate = jnp.zeros((8, 1), F32)
    for i in range(8):
        rate = jnp.where(r8 == i, rate_in[i // 4, t * 16 + f * 4 + i % 4], rate)
    rate = jnp.exp(rate)
    def pick(rows, which, n):
        chosen = rows[0:4]
        for i in range(1, n):
            chosen = jnp.where(which == i, rows[4 * i : 4 * i + 4], chosen)
        return chosen

    lds = []
    for o in range(4):
        s = slot_seq(o)
        w0, w1 = wst[:, :, 0:512].reshape(32, 512), wst[:, :, 512:1024].reshape(32, 512)
        all_raw = dot(w0, x_b[s, 0], ((1,), (1,))) + dot(w1, x_b[s, 1], ((1,), (1,)))
        raw = jnp.concatenate([pick(all_raw[0:16], f, 4), pick(all_raw[16:32], f, 4)], axis=0)
        odd = lax.rem(f, 2)
        extra = jnp.concatenate([pick(de[s, 0], odd, 2), pick(de[s, 1], odd, 2)], axis=0)
        stp = jnp.maximum(raw, 0.0) + jnp.log1p(jnp.exp(-jnp.abs(raw)))
        stp_s[o] = stp
        lds.append(extra - stp * rate)
    ld = jnp.concatenate(lds, axis=0)
    ld_a = ld.astype(BF16)
    rest = ld - ld_a.astype(F32)
    ld_b = rest.astype(BF16)
    ld_c = (rest - ld_b.astype(F32)).astype(BF16)
    ld3 = jnp.concatenate([ld_a, ld_b, ld_c], axis=0)
    pre = dot(ld3, (ii <= jj).astype(F32).astype(BF16))
    suf = dot(ld3, (ii >= jj).astype(F32).astype(BF16))
    pre = pre[0:32] + (pre[32:64] + pre[64:96])
    suf = suf[0:32] + (suf[32:64] + suf[64:96])
    fwd_row = lax.rem(lax.broadcasted_iota(jnp.int32, (32, T), 0), 8) < 4
    cum = jnp.where(fwd_row, pre, suf)
    cum_s[...] = cum.reshape(4, 8, T)
    lane4 = lax.broadcasted_iota(jnp.int32, (1, 256), 1) // 64
    ends = []
    for o in range(4):
        for r in range(2):
            row = jnp.zeros((1, 256), F32)
            for h in range(4):
                i = o * 8 + r * 4 + h
                e = cum[i : i + 1, T - 1 : T] if r == 0 else cum[i : i + 1, 0:1]
                row = jnp.where(lane4 == h, e, row)
            ends.append(row)
    dec[...] = jnp.concatenate(ends, axis=0)
    own_dec = local(dec, d1.at[y])
    sd1 = [send(dec, d1.at[y], {"y": ymod(d)}) for d in near_first]

    halo_local.wait()
    for c in halos:
        c.wait_recv()
    zr[3].wait_recv()
    yr[3].wait_recv()

    def rows_of(w, k, n):
        return w[4 * k : 4 * k + 4].reshape(512, n)

    h0 = hall[:, 0].reshape(128, 512)
    h1 = hall[:, 1].reshape(128, 512)
    side = lax.rem(lax.broadcasted_iota(jnp.int32, (128, 256), 0) // 16, 2)
    gone = jnp.logical_or(
        jnp.logical_and(side == 0, sp == 0), jnp.logical_and(side == 1, sp == 63)
    )
    for i, w in enumerate((wa1, wa2)):
        hproj = (dot(h0, rows_of(w, 0, 256)) + dot(h1, rows_of(w, 1, 256))).astype(BF16).astype(F32)
        hp[:, :, :, i * 256 : (i + 1) * 256] = jnp.where(gone, 0.0, hproj).reshape(4, 2, 16, 256)

    def spread(cols, c):
        parts = [
            jnp.where(low, cols[:, c + 2 * q : c + 2 * q + 1], cols[:, c + 2 * q + 1 : c + 2 * q + 2])
            for q in range(2)
        ]
        return jnp.concatenate(parts, axis=1)

    def front(o, hf):
        s = slot_seq(o)
        x0, x1 = x_b[s, 0], x_b[s, 1]
        for i, w in enumerate((wa1, wa2)):
            pa = dot(x0, rows_of(w, 0, 256)) + dot(x1, rows_of(w, 1, 256))
            p_s[16:272, i * 256 : (i + 1) * 256] = pa.astype(BF16).astype(F32)
        p_s[0:16, :] = hp[s, 0]
        p_s[272:288, :] = hp[s, 1]
        conv = p_s[14 : 14 + T, :] * par[0:1, :]
        for j in range(1, 5):
            conv = conv + p_s[14 + j : 14 + j + T, :] * par[j : j + 1, :]
        act = silu(conv)
        v, b, c = act[:, 0:256], act[:, 256:384], act[:, 384:512]
        cols = jnp.concatenate([cum_s[o], stp_s[o], jnp.zeros((112, T), F32)], axis=0).T
        cols_s[o] = cols
        v_s[o] = v.astype(BF16)
        b_s[o] = b.astype(BF16)
        c_s[o] = c.astype(BF16)
        bt = b.T.astype(BF16)
        lane = lax.broadcasted_iota(jnp.int32, (1, 128), 1)
        end = jnp.where(lane < 4, cols[T - 1 : T, :], cols[0:1, :])
        w_end = jnp.exp(end - cols)
        n = (o - 2 * hf) * 2
        for r in range(2):
            scale = spread(w_end, 4 * r) * spread(cols, 8 + 4 * r)
            st[hf, :, n + r] = dot(bt, (v * scale).astype(BF16)).astype(BF16).reshape(8, 16, 256)

    s1, own_st = [], []
    for hf in range(2):

        def front_step(o, _, hf=hf):
            front(o, hf)
            return _

        lax.fori_loop(2 * hf, 2 * hf + 2, front_step, 0)
        own_st.append(local(st.at[hf, y], r1.at[hf, y]))
        s1.append([send(st.at[hf, ymod(d)], r1.at[hf, y], {"y": ymod(d)}) for d in near_first])
        gate_step(hf + 1)
        if hf == 0:
            own_dec.wait()
            for c in sd1:
                c.wait_recv()
            cumf = jnp.zeros((8, 256), F32)
            cumb = jnp.zeros((8, 256), F32)
            back = lax.rem(lax.broadcasted_iota(jnp.int32, (8, 256), 0), 2) == 1
            pf = []
            for i in range(8):
                pf.append(cumf)
                cumf = cumf + d1[i]
            for i in reversed(range(8)):
                pd[i] = jnp.exp(jnp.where(back, cumb, pf[i]))
                cumb = cumb + d1[i]
            totd[...] = cumf
            own_td = local(totd, d2.at[z])
            sd2 = [send(totd, d2.at[z], {"z": zmod(d)}) for d in near_first]

    def inner(o, _):
        cols, cu, stp = cols_s[o], cum_s[o], stp_s[o]
        scores = dot(c_s[o], b_s[o], ((1,), (1,)))
        for q in range(2):
            vp = v_s[o, :, q * 128 : (q + 1) * 128]
            both = []
            for e in range(2):
                h = 2 * q + e
                expo = jnp.where(
                    jj <= ii,
                    cols[:, h : h + 1] - cu[h : h + 1, :],
                    cols[:, 4 + h : 5 + h] - cu[4 + h : 5 + h, :],
                )
                df, db = stp[h : h + 1, :], stp[4 + h : 5 + h, :]
                dts = jnp.where(jj < ii, df, jnp.where(jj > ii, db, df + db))
                both.append(dot((scores * jnp.exp(expo) * dts).astype(BF16), vp))
            y_s[o, :, q * 128 : (q + 1) * 128] = jnp.where(low, both[0], both[1])
        return _

    def scan1(hf):
        own_st[hf].wait()
        for c in s1[hf]:
            c.wait_recv()
        for n in range(4):
            run = jnp.zeros((16, 256), F32)
            for i in range(8) if n % 2 == 0 else reversed(range(8)):
                res[hf, i, n] = run
                w = jnp.exp(d1[i, 4 * hf + n : 4 * hf + n + 1, :])
                run = run * w + r1[hf, i, n].astype(F32)
            tot[hf, n] = run.astype(BF16)
        mine = local(tot.at[hf], r2.at[hf, z])
        return mine, [send(tot.at[hf], r2.at[hf, z], {"z": zmod(d)}) for d in near_first]

    def scan2(hf, s2):
        s2[0].wait()
        for c in s2[1]:
            c.wait_recv()
        for n in range(4):
            acc = jnp.zeros((16, 256), F32)
            for i in range(8) if n % 2 == 0 else reversed(range(8)):
                w = jnp.exp(d2[i, 4 * hf + n : 4 * hf + n + 1, :])
                new = acc * w + r2[hf, i, n].astype(F32)
                used = (i < z) if n % 2 == 0 else (i > z)
                acc = jnp.where(used, new, acc)
            for i in range(8):
                w = pd[i, 4 * hf + n : 4 * hf + n + 1, :]
                r1[hf, i, n] = (res[hf, i, n] + acc * w).astype(BF16)
        mine = local(r1.at[hf, y], inc.at[hf, y])
        return mine, [send(r1.at[hf, ymod(d)], inc.at[hf, y], {"y": ymod(d)}) for d in near_first]

    lax.fori_loop(0, 2, inner, 0)
    s2_0 = scan1(0)
    gate_step(3)

    gate_step(4)

    def gates(o, _):
        s = slot_seq(o)
        x0, x1 = x_b[s, 0], x_b[s, 1]
        g = dot(x0, rows_of(wb1, 0, 256)) + dot(x1, rows_of(wb1, 1, 256))
        gate[o] = silu(g.astype(BF16).astype(F32))
        q = dot(x0, rows_of(wb2, 0, 128)) + dot(x1, rows_of(wb2, 1, 128))
        pool[1, o] = q.astype(BF16)
        return _

    lax.fori_loop(0, 4, gates, 0)

    def pool_copies(g):
        n = GRID_W << g
        spans = ((T - n, 0, 0, nxt), (0, 2, 1, prv))
        return [
            pltpu.make_async_remote_copy(
                src_ref=pool.at[1, :, pl.ds(a, n)], dst_ref=pool.at[b, :, pl.ds(a, n)],
                send_sem=psem.at[0, i], recv_sem=psem.at[1, i], device_id=dev, device_id_type=MESH,
            )
            for a, b, i, dev in spans
        ]

    for g in range(4):

        @pl.when(group_at == g)
        def _():
            for c in pool_copies(g):
                c.start()

    s2_1 = scan1(1)
    own_td.wait()
    for c in sd2:
        c.wait_recv()
    s3_0 = scan2(0, s2_0)
    wos = []
    for d in (1, 3, 2):
        g = fmod(d)
        wos.append(send(woi_in.at[at(g, 256)], woi.at[f], {"fs": g}))
        wos.append(send(wop_in.at[at(g // 2, 256)], wop.at[f], {"fs": g}))
    lax.fori_loop(2, 4, inner, 0)
    s3_1 = scan2(1, s2_1)

    k = jnp.left_shift(jnp.int32(2), group_at)
    ti = lax.broadcasted_iota(jnp.int32, (T, 3 * T), 0)
    tj = lax.broadcasted_iota(jnp.int32, (T, 3 * T), 1)
    ri, ci_ = ti // GRID_W + 8, lax.rem(ti, GRID_W)
    rj, cj = tj // GRID_W, lax.rem(tj, GRID_W)
    grow = rj + (sp * 8 - 8)
    inside = (rj >= ri - k // 2) & (rj < ri + k // 2) & (cj >= ci_ - k // 2) & (cj < ci_ + k // 2)
    inside = inside & (grow >= 0) & (grow < 512)
    m_s[...] = inside.astype(F32).astype(BF16)
    for g in range(4):

        @pl.when(group_at == g)
        def _():
            for c in pool_copies(g):
                c.wait()
    row = lax.broadcasted_iota(jnp.int32, (T, 128), 0) // GRID_W + sp * 8
    col = lax.rem(lax.broadcasted_iota(jnp.int32, (T, 128), 0), GRID_W)
    cells = (
        (jnp.minimum(row + k // 2, 512) - jnp.maximum(row - k // 2, 0))
        * (jnp.minimum(col + k // 2, GRID_W) - jnp.maximum(col - k // 2, 0))
    ).astype(F32)
    pgain = jnp.concatenate([pg[pl.ds(2 * group_at + i, 1), :] for i in range(2)], axis=1)
    ngain = jnp.concatenate([ng[pl.ds(8 * t + 2 * f + i, 1), :] for i in range(2)], axis=1)

    def pools(o, _):
        rows = jnp.concatenate([pool[0, o], pool[1, o], pool[2, o]], axis=0)
        off = dot(m_s[...], rows) / cells - pool[1, o].astype(F32)
        pld_s[o] = (dot(off.astype(BF16), pmix[...]) * pgain).astype(BF16)
        return _

    lax.fori_loop(0, 4, pools, 0)

    for c in wos:
        c.wait_recv()
    blk = ((ii // 64 == jj // 64).astype(F32) * (1.0 / 64.0)).astype(BF16)

    def finish(o):
        hf, n = o // 2, (o % 2) * 2
        cb, cols = c_s[o], jnp.exp(cols_s[o])
        carried = dot(cb, inc[hf, :, n].reshape(128, 256)) * spread(cols, 0)
        carried = carried + dot(cb, inc[hf, :, n + 1].reshape(128, 256)) * spread(cols, 4)
        g = (y_s[o] + carried) * gate[o]
        ms = dot((g * g).astype(BF16), blk)
        mix_s[...] = (g * lax.rsqrt(ms + EPSILON) * ngain).astype(BF16)

    mine = at(t, 128)
    theirs = at(1 - t, 128)
    far = []
    for o in range(4):
        if o % 2 == 0:
            s3 = s3_0 if o == 0 else s3_1
            s3[0].wait()
            for c in s3[1]:
                c.wait_recv()
        finish(o)
        for q in range(4):
            cs = slice(q * 256, (q + 1) * 256)
            part = dot(mix_s[theirs, :], woi[q]) + dot(pld_s[o, theirs, :], wop[q])
            dsend[o, :, cs] = part.astype(BF16)
        swap = send(dsend.at[o], drecv.at[o], pair)
        for q in range(4):
            cs = slice(q * 256, (q + 1) * 256)
            own[o, :, cs] = dot(mix_s[mine, :], woi[q]) + dot(pld_s[o, mine, :], wop[q])
        swap.wait_recv()
        chip = own[o] + drecv[o].astype(F32)
        if o == 0:
            raws[...] = chip.astype(BF16).reshape(2, 64, 1024)
            up = send(raws.at[0], rawr.at[0], {"fs": fmod(1)})
            down = send(raws.at[1], rawr.at[1], {"fs": fmod(3)})
        elif o == 1:
            up.wait_recv()
            xsend[0, 0:64] = (chip[0:64] + rawr[0].astype(F32)).astype(BF16)
            xsend[0, 64:128] = chip[64:128].astype(BF16)
            far.append(send(xsend.at[0], xrecv.at[0], {"fs": fmod(1)}))
        elif o == 2:
            down.wait_recv()
            xsend[1, 0:64] = chip[0:64].astype(BF16)
            xsend[1, 64:128] = (chip[64:128] + rawr[1].astype(F32)).astype(BF16)
            far.append(send(xsend.at[1], xrecv.at[1], {"fs": fmod(3)}))
        else:
            own[o] = chip
    for c in far:
        c.wait_recv()
    out[0] = (own[3] + xrecv[0].astype(F32) + xrecv[1].astype(F32)).astype(BF16)
    for c in sent:
        c.wait_send()


N_REMOTE = 150


def body(
    tokens, w_inner, w_gate, w_write, w_read, w_pool_in, w_step, conv_inner, conv_cross, rate_log,
    decay_extra, norm_gain, pool_mix, pool_gain, w_out_inner, w_out_pool,
):
    hbm = pl.BlockSpec(memory_space=pl.ANY)
    V = pltpu.VMEM
    scratch = [
        V((4, 2, T, 512), BF16),
        V((2, 16, 512), BF16),
        V((4, 2, 2, 16, 512), BF16),
        V((8, 8, 16, 256), BF16),
        V((8, 8, 16, 256), BF16),
        V((8, 8, 16, 256), BF16),
        V((8, 8, 16, 128), BF16),
        V((4, 256, 256), BF16),
        V((4, 256, 256), BF16),
        V((4, 2, 8, T), F32),
        V((128, 256), BF16),
        V((2, 16, 1024), BF16),
        V((5, 256), BF16),
        V((5, 2, 128), BF16),
        V((16, 128), F32),
        V((8, 128), F32),
        V((8, 512), F32),
        V((288, 512), F32),
        V((4, 2, 16, 512), F32),
        V((4, T, 256), F32),
        V((4, T, 256), BF16),
        V((4, T, 128), BF16),
        V((4, T, 128), BF16),
        V((4, 8, T), F32),
        V((4, 8, T), F32),
        V((4, T, 128), F32),
        V((4, T, 256), F32),
        V((3, 4, T, 128), BF16),
        V((T, 3 * T), BF16),
        V((2, 8, 4, 16, 256), BF16),
        V((8, 256), F32),
        V((2, 8, 4, 16, 256), BF16),
        V((8, 8, 256), F32),
        V((8, 8, 256), F32),
        V((2, 8, 4, 16, 256), BF16),
        V((8, 8, 256), F32),
        V((8, 256), F32),
        V((2, 8, 4, 16, 256), F32),
        V((2, 4, 16, 256), BF16),
        V((2, 8, 4, 16, 256), BF16),
        V((4, 128, 1024), F32),
        V((4, 128, 1024), BF16),
        V((4, 128, 1024), BF16),
        V((2, 64, 1024), BF16),
        V((2, 64, 1024), BF16),
        V((2, 128, 1024), BF16),
        V((2, 128, 1024), BF16),
        V((T, 256), BF16),
        V((4, T, 256), BF16),
        pltpu.SemaphoreType.DMA((32,)),
        pltpu.SemaphoreType.DMA((N_REMOTE,)),
        pltpu.SemaphoreType.DMA((N_REMOTE,)),
        pltpu.SemaphoreType.DMA((2, 2)),
    ]
    return pl.pallas_call(
        kernel,
        out_shape=jax.ShapeDtypeStruct((1, 128, 1024), BF16),
        in_specs=[hbm] * 9 + [pl.BlockSpec(memory_space=pltpu.SMEM)] + [hbm] * 6,
        out_specs=pl.BlockSpec(memory_space=pltpu.VMEM),
        scratch_shapes=scratch,
        compiler_params=pltpu.CompilerParams(
            collective_id=0, has_side_effects=True, vmem_limit_bytes=60 * 1024 * 1024
        ),
    )(
        tokens, w_inner, w_gate, w_write, w_read, w_pool_in, jnp.transpose(w_step, (1, 2, 0)),
        conv_inner, conv_cross, rate_log, jnp.transpose(decay_extra[0], (1, 2, 0)),
        norm_gain.reshape(16, 128), pool_mix, pool_gain.reshape(8, 128), w_out_inner, w_out_pool,
    )


def solution(mesh):
    finer = Mesh(
        mesh.devices.reshape(8, 8, mesh.shape["fs"], mesh.shape["tp"]), ("z", "y", "fs", "tp")
    )
    in_specs = (
        P("fs", SP, "tp"),
        P(SP, "tp"),
        P(SP, "tp"),
        P(SP, "tp"),
        P(SP, "tp"),
        P(SP, "tp"),
        P(),
        P(),
        P(),
        P(),
        P("fs", SP, None, "tp"),
        P(),
        P(),
        P(),
        P("tp", "fs"),
        P("tp", "fs"),
    )
    out_specs = P("fs", ("z", "y", "tp"), None)
    return jax.shard_map(body, mesh=finer, in_specs=in_specs, out_specs=out_specs, check_vma=False)
```

time: 132 us -> 96.2 us (0.73)
  Pallas kernels: 124 us -> 94.3 us
  local copies, waits for them, and re-layouts: 6.87 us -> 1.67 us
    pallas_call x1, Pallas kernels: 124 us -> 94.3 us  [body(): pl.pallas_call(kernel, out_shape=jax.ShapeDtypeStruct((1, 128, 1024), BF1...]
    dynamic_slice x5 -> x0, local copies, waits for them, and re-layouts: 2.27 us -> none  [the longest x1 0.79 us: body(): cut(pool_gain, group * 256, 256, 0)]
where the time goes in v2:
time: 96.2 us; the launch traced here: 96 us
  Pallas kernels  94.3 us (98%)
  local copies, waits for them, and re-layouts  1.67 us (2%)
    pallas_call x1, Pallas kernels, body(): pl.pallas_call(kernel, out_shape=jax.ShapeDtypeStruct((1, 128, 1024), BF1...  94.3 us

profile of v2, /device:TPU:1, one launch (start us, length us, event | category | flops | bytes accessed | tf_op | source)
XLA Modules:
  0.0 96.0 jit_solution(11415157092452623878)
XLA Ops:
  0.0 94.3 %shard_map.154 = bf16[1,128,1024]{2,1,0:T(8,128)(2,1)} custom-call(bf16[1,256,512]{2,1,0:T(8,128)(2,1)} %tok.1, bf16[16,1024]{1,0:T(8,128)(2,1)} %w_inner.1, bf16[16,1024]{1,0:T(8,128)(2,1)} %w_gate.1, bf16[16,256]{1,0:T(8,128)(2,1)} %w_write.1, bf16[16,256]{1,0:T(8,128)(2,1)} %w_read.1, bf16[16,512]{1,0:T(8,128)(2,1)} %w_pool.1, ...), custom_call_target="tpu_custom_call" | custom-call | tf_op jit(solution)/shard_map/pallas_call | solution.py:577
  94.3 1.7 %copy.18 = bf16[1,128,1024]{2,1,0:T(8,128)(2,1)} copy(bf16[1,128,1024]{2,1,0:T(8,128)(2,1)} %shard_map.154) | data formatting | bytes 524288

commit v3 on v2

v3 whole, which is shorter than its diff:
```python
import functools

import jax
import jax.numpy as jnp
from jax import lax
from jax.experimental import pallas as pl
from jax.experimental.pallas import tpu as pltpu
from jax.sharding import Mesh
from jax.sharding import PartitionSpec as P

MESH = pl.DeviceIdType.MESH
F32, BF16 = jnp.float32, jnp.bfloat16
SP = ("z", "y")
EPSILON = 1e-05
T = 256
GRID_W = 32


def silu(v):
    return (0.5 * v) * (1.0 + jnp.tanh(0.5 * v))


def dot(a, b, dims=((1,), (0,)), **kw):
    return lax.dot_general(a, b, (dims, ((), ())), preferred_element_type=F32, **kw)


def kernel(
    tok, w_inner, w_gate, w_write, w_read, w_pool, wst_in, ci_in, cc_in, rate_in, dec_in, ng_in, pmix_in,
    pg_in, woi_in, wop_in,
    out,
    x_b, hrow, hall, wa1, wa2, wb1, wb2, alt1, alt3, alt4, woi, wop, de, pmix, wst, ci, cc, ng, pg, par,
    p_s, hp, y_s, v_s, b_s, c_s, cum_s, stp_s, cols_s, gate, pool, m_s,
    sb, dec, decp, st, r1, d1, pd, r2, d2, totd, res, tot, inc, b_in, own, dsend, drecv, raws, rawr, xsend, xrecv,
    mix_s, pld_s,
    lsem, ssem, rsem, psem,
):
    z, y, f, t = (lax.axis_index(a) for a in ("z", "y", "fs", "tp"))
    fq, yq, yp = lax.rem(f, 2), lax.rem(y, 2), y // 2
    r = fq * 2 + yq
    sp = z * 8 + y
    group_at = t * 2 + fq

    def along(d):
        v = lax.rem(sp + d, 64)
        return {"z": v // 8, "y": lax.rem(v, 8)}

    count = [0, 0]
    sent = []

    def send(src, dst, dev):
        i = count[0]
        count[0] += 1
        c = pltpu.make_async_remote_copy(
            src_ref=src, dst_ref=dst, send_sem=ssem.at[i], recv_sem=rsem.at[i],
            device_id=dev, device_id_type=MESH,
        )
        c.start()
        sent.append(c)
        return c

    def local(src, dst):
        c = pltpu.make_async_copy(src, dst, lsem.at[count[1]])
        count[1] += 1
        c.start()
        return c

    def ymod(d):
        return lax.rem(y + d, 8)

    def zmod(d):
        return lax.rem(z + d, 8)

    def fmod(d):
        return lax.rem(f + d, 4)

    def pmod(d):
        return lax.rem(yp + d, 4)

    f_flip, y_flip = f + 1 - 2 * fq, y + 1 - 2 * yq
    r_x, r_y, r_d = (1 - fq) * 2 + yq, fq * 2 + 1 - yq, 3 - r
    to_x, to_y, to_d = {"fs": f_flip}, {"y": y_flip}, {"fs": f_flip, "y": y_flip}

    def at(v, n):
        return pl.ds(pl.multiple_of(v * n, n), n)

    near_first = (1, 7, 2, 6, 3, 5, 4)
    pair = {"tp": 1 - t}
    group = [pair] + [{**a, "tp": e} for a in (to_x, to_y, to_d) for e in (t, 1 - t)]
    peers = [{"y": ymod(d)} for d in range(1, 8)] + [{"z": zmod(d)} for d in range(1, 8)]
    peers += group + [{"fs": fmod(d)} for d in range(1, 4)] + [along(d) for d in (1, 63, 2, 62)]

    pool[:, 0] = jnp.zeros((2, T, 128), BF16)
    pool[:, 3] = jnp.zeros((2, T, 128), BF16)
    barrier = pltpu.get_barrier_semaphore()
    for p in peers:
        pl.semaphore_signal(barrier, inc=1, device_id=p, device_id_type=MESH)
    mine1, mine2, mine3, mine4 = (w.at[z, y] for w in (wa1, wa2, wb1, wb2))
    tok_local = local(tok.at[0], x_b.at[r, t])
    w_local = [
        local(w_inner.at[:, at(r, 256)], mine1),
        local(w_inner.at[:, at(r_y, 256)], alt1),
        local(w_write.at[:, at(fq, 128)], mine2.at[:, pl.ds(0, 128)]),
        local(w_read.at[:, at(fq, 128)], mine2.at[:, pl.ds(128, 128)]),
        local(w_gate.at[:, at(r, 256)], mine3),
        local(w_gate.at[:, at(r_y, 256)], alt3),
        local(w_pool.at[:, at(r, 128)], mine4),
        local(w_pool.at[:, at(r_y, 128)], alt4),
    ]
    others = [
        local(wst_in.at[:, at(t, 16)], wst),
        local(dec_in.at[:, at(fq, 8)], de.at[r]),
        local(ci_in.at[:, at(t * 4 + r, 256)], ci),
        local(cc_in.at[:, :, at(group_at, 128)], cc),
        local(ng_in, ng),
        local(pg_in, pg),
        local(pmix_in.at[group_at, at(yq, 128)], pmix),
        local(woi_in.at[at(r, 256)], woi.at[f]),
        local(wop_in.at[at(fq, 256)], wop.at[f]),
    ]
    tok_local.wait()
    for c in w_local:
        c.wait()
    pl.semaphore_wait(barrier, len(peers))

    x_own = x_b.at[r, t]
    edge_n = send(x_own.at[pl.ds(240, 16)], hrow.at[0], along(1))
    edge_p = send(x_own.at[pl.ds(0, 16)], hrow.at[1], along(63))

    def stage(mine, alt):
        return [send(alt if d % 2 else mine, mine, {"y": ymod(d)}) for d in near_first]

    first, second = stage(mine1, alt1), stage(mine2, mine2)
    x_right = send(x_own, x_own, to_x)
    x_left = send(x_own, x_own, to_y)
    x_pair = [send(x_own, x_own, pair)]
    decs = [
        send(dec_in.at[:, at(q, 8)], de.at[r], g)
        for q, g in ((1 - fq, to_x), (fq, to_y), (1 - fq, to_d))
    ]
    third, fourth = stage(mine3, alt3), stage(mine4, alt4)

    def ring_z(w, k, to):
        s = w.at[zmod(8 - k if to == 1 else k)]
        if k == 3:
            s = s.at[pl.ds(0 if to == 1 else 4, 4)]
        return send(s, s, {"z": zmod(to)})

    rings = {}

    def begin(name, w):
        rings[name] = [(w, to, [ring_z(w, 0, to)]) for to in (1, 7)]

    def step(names, k):
        for name in names:
            for w, to, ring in rings[name]:
                ring[k - 1].wait_recv()
                if k < 4:
                    ring.append(ring_z(w, k, to))

    for c in first:
        c.wait_recv()
    begin("a1", wa1)
    for c in second:
        c.wait_recv()
    begin("a2", wa2)
    edge_n.wait_recv()
    edge_p.wait_recv()
    halo_local = local(hrow, hall.at[r, t])
    halos = [send(hrow, hall.at[r, t], g) for g in group]
    step(("a1", "a2"), 1)
    x_right.wait_recv()
    block = x_b.at[r_x, t]
    x_fr = send(block.at[pl.ds(0, 128)], block.at[pl.ds(0, 128)], to_y)
    x_pair.append(send(block, block, pair))
    x_left.wait_recv()
    block = x_b.at[r_y, t]
    x_fl = send(block.at[pl.ds(128, 128)], block.at[pl.ds(128, 128)], to_x)
    x_pair.append(send(block, block, pair))
    step(("a1", "a2"), 2)
    for c in others:
        c.wait()
    par[0:5, 0:256] = ci[...].astype(F32)
    par[0:5, 256:384] = cc[:, 0, :].astype(F32)
    par[0:5, 384:512] = cc[:, 1, :].astype(F32)
    x_fr.wait_recv()
    x_fl.wait_recv()
    block = x_b.at[r_d, t]
    x_pair.append(send(block, block, pair))
    step(("a1", "a2"), 3)
    for c in third + fourth:
        c.wait_recv()
    begin("b1", wb1)
    begin("b2", wb2)
    wos = []
    for d in (1, 3, 2):
        g = fmod(d)
        q = lax.rem(g, 2)
        wos.append(send(woi_in.at[at(q * 2 + yq, 256)], woi.at[f], {"fs": g}))
        wos.append(send(wop_in.at[at(q, 256)], wop.at[f], {"fs": g}))

    def gate_step(k):
        step(("b1", "b2"), k)

    for c in x_pair + decs:
        c.wait_recv()
    ii = lax.broadcasted_iota(jnp.int32, (T, T), 0)
    jj = lax.broadcasted_iota(jnp.int32, (T, T), 1)
    low = lax.broadcasted_iota(jnp.int32, (T, 128), 1) < 64

    def slot_block(o):
        return lax.rem(yq + lax.rem(3 - o, 2), 2)

    def slot_unit(o):
        return lax.rem(fq + (3 - o) // 2, 2) * 2 + slot_block(o)

    r8 = lax.broadcasted_iota(jnp.int32, (8, 1), 0)
    rate = jnp.zeros((8, 1), F32)
    for i in range(8):
        rate = jnp.where(r8 == i, rate_in[i // 4, t * 16 + r * 4 + i % 4], rate)
    rate = jnp.exp(rate)
    def pick(rows, which, n):
        chosen = rows[0:4]
        for i in range(1, n):
            chosen = jnp.where(which == i, rows[4 * i : 4 * i + 4], chosen)
        return chosen

    lds = []
    for o in range(4):
        s = slot_unit(o)
        w0, w1 = wst[:, :, 0:512].reshape(32, 512), wst[:, :, 512:1024].reshape(32, 512)
        all_raw = dot(w0, x_b[s, 0], ((1,), (1,))) + dot(w1, x_b[s, 1], ((1,), (1,)))
        raw = jnp.concatenate([pick(all_raw[0:16], r, 4), pick(all_raw[16:32], r, 4)], axis=0)
        extra = jnp.concatenate([pick(de[s, 0], yq, 2), pick(de[s, 1], yq, 2)], axis=0)
        stp = jnp.maximum(raw, 0.0) + jnp.log1p(jnp.exp(-jnp.abs(raw)))
        stp_s[o] = stp
        lds.append(extra - stp * rate)
    ld = jnp.concatenate(lds, axis=0)
    ld_a = ld.astype(BF16)
    rest = ld - ld_a.astype(F32)
    ld_b = rest.astype(BF16)
    ld_c = (rest - ld_b.astype(F32)).astype(BF16)
    ld3 = jnp.concatenate([ld_a, ld_b, ld_c], axis=0)
    pre = dot(ld3, (ii <= jj).astype(F32).astype(BF16))
    suf = dot(ld3, (ii >= jj).astype(F32).astype(BF16))
    pre = pre[0:32] + (pre[32:64] + pre[64:96])
    suf = suf[0:32] + (suf[32:64] + suf[64:96])
    fwd_row = lax.rem(lax.broadcasted_iota(jnp.int32, (32, T), 0), 8) < 4
    cum = jnp.where(fwd_row, pre, suf)
    cum_s[...] = cum.reshape(4, 8, T)
    lane4 = lax.broadcasted_iota(jnp.int32, (1, 256), 1) // 64
    ends = []
    for o in range(4):
        for n in range(2):
            row = jnp.zeros((1, 256), F32)
            for h in range(4):
                i = o * 8 + n * 4 + h
                e = cum[i : i + 1, T - 1 : T] if n == 0 else cum[i : i + 1, 0:1]
                row = jnp.where(lane4 == h, e, row)
            ends.append(row)
    dec[...] = jnp.concatenate(ends, axis=0)
    both = [ends[4 * hf + n] + ends[4 * hf + 2 + n] for hf in range(2) for n in range(2)]
    decp[...] = jnp.concatenate(both + [jnp.zeros((4, 256), F32)], axis=0)
    own_dec = local(decp, d1.at[yp])
    sd1 = [send(decp, d1.at[yp], {"y": ymod(2 * d)}) for d in (1, 3, 2)]

    halo_local.wait()
    for c in halos:
        c.wait_recv()
    step(("a1", "a2"), 4)

    def rows_of(w, k, n):
        return w[4 * k : 4 * k + 4].reshape(512, n)

    h0 = hall[:, 0].reshape(128, 512)
    h1 = hall[:, 1].reshape(128, 512)
    hrow_at = lax.broadcasted_iota(jnp.int32, (128, 256), 0)
    side = lax.rem(hrow_at // 16, 2)
    place = sp - yq + lax.rem(hrow_at // 32, 2)
    gone = jnp.logical_or(
        jnp.logical_and(side == 0, place == 0), jnp.logical_and(side == 1, place == 63)
    )
    for i, w in enumerate((wa1, wa2)):
        hproj = (dot(h0, rows_of(w, 0, 256)) + dot(h1, rows_of(w, 1, 256))).astype(BF16).astype(F32)
        hp[:, :, :, i * 256 : (i + 1) * 256] = jnp.where(gone, 0.0, hproj).reshape(4, 2, 16, 256)

    def spread(cols, c):
        parts = [
            jnp.where(low, cols[:, c + 2 * q : c + 2 * q + 1], cols[:, c + 2 * q + 1 : c + 2 * q + 2])
            for q in range(2)
        ]
        return jnp.concatenate(parts, axis=1)

    def front(o):
        s = slot_unit(o)
        x0, x1 = x_b[s, 0], x_b[s, 1]
        for i, w in enumerate((wa1, wa2)):
            pa = dot(x0, rows_of(w, 0, 256)) + dot(x1, rows_of(w, 1, 256))
            p_s[16:272, i * 256 : (i + 1) * 256] = pa.astype(BF16).astype(F32)
        p_s[0:16, :] = hp[s, 0]
        p_s[272:288, :] = hp[s, 1]
        conv = p_s[14 : 14 + T, :] * par[0:1, :]
        for j in range(1, 5):
            conv = conv + p_s[14 + j : 14 + j + T, :] * par[j : j + 1, :]
        act = silu(conv)
        v, b, c = act[:, 0:256], act[:, 256:384], act[:, 384:512]
        cols = jnp.concatenate([cum_s[o], stp_s[o], jnp.zeros((112, T), F32)], axis=0).T
        cols_s[o] = cols
        v_s[o] = v.astype(BF16)
        b_s[o] = b.astype(BF16)
        c_s[o] = c.astype(BF16)
        bt = b.T.astype(BF16)
        lane = lax.broadcasted_iota(jnp.int32, (1, 128), 1)
        end = jnp.where(lane < 4, cols[T - 1 : T, :], cols[0:1, :])
        w_end = jnp.exp(end - cols)
        for n in range(2):
            scale = spread(w_end, 4 * n) * spread(cols, 8 + 4 * n)
            sb[o, n] = dot(bt, (v * scale).astype(BF16))

    def early_late(hf):
        return 2 * hf + 1 - yq, 2 * hf + yq

    def fade(o, n):
        return jnp.exp(dec[pl.ds(2 * o + n, 1), :])

    def join(hf):
        e, l = early_late(hf)
        ahead = sb[e, 0] * fade(l, 0) + sb[l, 0]
        behind = sb[l, 1] * fade(e, 1) + sb[e, 1]
        st[hf, :, 0] = ahead.astype(BF16).reshape(4, 32, 256)
        st[hf, :, 1] = behind.astype(BF16).reshape(4, 32, 256)

    def enter(hf):
        e, l = early_late(hf)
        ahead = inc[hf, :, 0].reshape(128, 256)
        behind = inc[hf, :, 1].reshape(128, 256)
        b_in[e, 0] = ahead
        b_in[l, 0] = (ahead.astype(F32) * fade(e, 0) + sb[e, 0]).astype(BF16)
        b_in[l, 1] = behind
        b_in[e, 1] = (behind.astype(F32) * fade(l, 1) + sb[l, 1]).astype(BF16)

    s1, own_st = [], []
    for hf in range(2):

        def front_step(o, _):
            front(o)
            return _

        lax.fori_loop(2 * hf, 2 * hf + 2, front_step, 0)
        join(hf)
        own_st.append(local(st.at[hf, yp], r1.at[hf, yp]))
        s1.append([send(st.at[hf, pmod(d)], r1.at[hf, yp], {"y": ymod(2 * d)}) for d in (1, 3, 2)])
        gate_step(hf + 1)
        if hf == 0:
            own_dec.wait()
            for c in sd1:
                c.wait_recv()
            cumf = jnp.zeros((8, 256), F32)
            cumb = jnp.zeros((8, 256), F32)
            back = lax.rem(lax.broadcasted_iota(jnp.int32, (8, 256), 0), 2) == 1
            pf = []
            for i in range(4):
                pf.append(cumf)
                cumf = cumf + d1[i]
            for i in reversed(range(4)):
                pd[i] = jnp.exp(jnp.where(back, cumb, pf[i]))
                cumb = cumb + d1[i]
            totd[...] = cumf
            sd2 = [send(totd, d2.at[z], {"z": zmod(d)}) for d in near_first]

    def inner(o, _):
        cols, cu, stp = cols_s[o], cum_s[o], stp_s[o]
        scores = dot(c_s[o], b_s[o], ((1,), (1,)))
        for q in range(2):
            vp = v_s[o, :, q * 128 : (q + 1) * 128]
            both = []
            for e in range(2):
                h = 2 * q + e
                expo = jnp.where(
                    jj <= ii,
                    cols[:, h : h + 1] - cu[h : h + 1, :],
                    cols[:, 4 + h : 5 + h] - cu[4 + h : 5 + h, :],
                )
                df, db = stp[h : h + 1, :], stp[4 + h : 5 + h, :]
                dts = jnp.where(jj < ii, df, jnp.where(jj > ii, db, df + db))
                both.append(dot((scores * jnp.exp(expo) * dts).astype(BF16), vp))
            y_s[o, :, q * 128 : (q + 1) * 128] = jnp.where(low, both[0], both[1])
        return _

    def scan1(hf):
        own_st[hf].wait()
        for c in s1[hf]:
            c.wait_recv()
        for n in range(2):
            run = jnp.zeros((32, 256), F32)
            for i in range(4) if n == 0 else reversed(range(4)):
                res[hf, i, n] = run
                w = jnp.exp(d1[i, 2 * hf + n : 2 * hf + n + 1, :])
                run = run * w + r1[hf, i, n].astype(F32)
            tot[hf, n] = run.astype(BF16)
        return [
            send(tot.at[hf, (z + d) // 8], r2.at[hf, z, (z + d) // 8], {"z": zmod(d)})
            for d in near_first
        ]

    def scan2(hf, s2):
        for c in s2:
            c.wait_recv()
        for n in range(2):
            acc = jnp.zeros((32, 256), F32)
            for i in range(8) if n == 0 else reversed(range(8)):
                w = jnp.exp(d2[i, 2 * hf + n : 2 * hf + n + 1, :])
                new = acc * w + r2[hf, i, n].astype(F32)
                used = (i < z) if n == 0 else (i > z)
                acc = jnp.where(used, new, acc)
            for i in range(4):
                w = pd[i, 2 * hf + n : 2 * hf + n + 1, :]
                r1[hf, i, n] = (res[hf, i, n] + acc * w).astype(BF16)
        mine = local(r1.at[hf, yp], inc.at[hf, yp])
        return mine, [
            send(r1.at[hf, pmod(d)], inc.at[hf, yp], {"y": ymod(2 * d)}) for d in (1, 3, 2)
        ]

    def gates(o, _):
        s = slot_unit(o)
        x0, x1 = x_b[s, 0], x_b[s, 1]
        g = dot(x0, rows_of(wb1, 0, 256)) + dot(x1, rows_of(wb1, 1, 256))
        gate[o] = silu(g.astype(BF16).astype(F32))
        q = dot(x0, rows_of(wb2, 0, 128)) + dot(x1, rows_of(wb2, 1, 128))
        pool[o // 2, 1 + slot_block(o)] = q.astype(BF16)
        return _

    def pool_copies(g):
        n = GRID_W << g
        spans = ((2, 0, T - n, along(2)), (1, 3, 0, along(62)))
        return [
            pltpu.make_async_remote_copy(
                src_ref=pool.at[:, a, pl.ds(c, n)], dst_ref=pool.at[:, b, pl.ds(c, n)],
                send_sem=psem.at[0, i], recv_sem=psem.at[1, i], device_id=dev, device_id_type=MESH,
            )
            for i, (a, b, c, dev) in enumerate(spans)
        ]

    lax.fori_loop(0, 2, inner, 0)
    gate_step(3)
    s2_0 = scan1(0)
    lax.fori_loop(2, 4, inner, 0)
    gate_step(4)
    s2_1 = scan1(1)
    for c in sd2:
        c.wait_recv()
    s3_0 = scan2(0, s2_0)
    lax.fori_loop(0, 4, gates, 0)
    for g in range(4):

        @pl.when(group_at == g)
        def _():
            for c in pool_copies(g):
                c.start()

    s3_1 = scan2(1, s2_1)

    k = jnp.left_shift(jnp.int32(2), group_at)
    ti = lax.broadcasted_iota(jnp.int32, (T, 3 * T), 0)
    tj = lax.broadcasted_iota(jnp.int32, (T, 3 * T), 1)
    ri, ci_ = ti // GRID_W + 8, lax.rem(ti, GRID_W)
    rj, cj = tj // GRID_W, lax.rem(tj, GRID_W)
    inside = (rj >= ri - k // 2) & (rj < ri + k // 2) & (cj >= ci_ - k // 2) & (cj < ci_ + k // 2)
    m_s[...] = inside.astype(F32).astype(BF16)
    for g in range(4):

        @pl.when(group_at == g)
        def _():
            for c in pool_copies(g):
                c.wait()
    pool[:, 0] = jnp.where(sp // 2 == 0, jnp.zeros((2, T, 128), BF16), pool[:, 0])
    pool[:, 3] = jnp.where(sp // 2 == 31, jnp.zeros((2, T, 128), BF16), pool[:, 3])
    col = lax.rem(lax.broadcasted_iota(jnp.int32, (T, 128), 0), GRID_W)
    cols_in = jnp.minimum(col + k // 2, GRID_W) - jnp.maximum(col - k // 2, 0)
    pgain = jnp.concatenate([pg[pl.ds(2 * group_at + i, 1), :] for i in range(2)], axis=1)
    ngain = jnp.concatenate([ng[pl.ds(8 * t + 2 * r + i, 1), :] for i in range(2)], axis=1)

    def pools(o, _):
        b = slot_block(o)
        row = lax.broadcasted_iota(jnp.int32, (T, 128), 0) // GRID_W + (sp - yq + b) * 8
        cells = (jnp.minimum(row + k // 2, 512) - jnp.maximum(row - k // 2, 0)) * cols_in
        rows = jnp.concatenate([pool[o // 2, b + i] for i in range(3)], axis=0)
        off = dot(m_s[...], rows) / cells.astype(F32) - pool[o // 2, b + 1].astype(F32)
        pld_s[o] = (dot(off.astype(BF16), pmix[...]) * pgain).astype(BF16)
        return _

    lax.fori_loop(0, 4, pools, 0)

    for c in wos:
        c.wait_recv()
    blk = ((ii // 64 == jj // 64).astype(F32) * (1.0 / 64.0)).astype(BF16)

    def finish(o):
        cb, cols = c_s[o], jnp.exp(cols_s[o])
        carried = dot(cb, b_in[o, 0]) * spread(cols, 0) + dot(cb, b_in[o, 1]) * spread(cols, 4)
        g = (y_s[o] + carried) * gate[o]
        ms = dot((g * g).astype(BF16), blk)
        mix_s[...] = (g * lax.rsqrt(ms + EPSILON) * ngain).astype(BF16)

    mine = at(t, 128)
    theirs = at(1 - t, 128)
    far = []
    for o in range(4):
        if o % 2 == 0:
            s3 = s3_0 if o == 0 else s3_1
            s3[0].wait()
            for c in s3[1]:
                c.wait_recv()
            enter(o // 2)
        finish(o)
        for q in range(4):
            cs = slice(q * 256, (q + 1) * 256)
            part = dot(mix_s[theirs, :], woi[q]) + dot(pld_s[o, theirs, :], wop[q])
            dsend[o, :, cs] = part.astype(BF16)
        swap = send(dsend.at[o], drecv.at[o], pair)
        for q in range(4):
            cs = slice(q * 256, (q + 1) * 256)
            own[o, :, cs] = dot(mix_s[mine, :], woi[q]) + dot(pld_s[o, mine, :], wop[q])
        swap.wait_recv()
        chip = own[o] + drecv[o].astype(F32)
        if o == 0:
            raws[...] = chip.astype(BF16).reshape(2, 64, 1024)
            up = send(raws.at[0], rawr.at[0], to_x)
            down = send(raws.at[1], rawr.at[1], to_y)
        elif o == 1:
            down.wait_recv()
            xsend[0, 0:64] = chip[0:64].astype(BF16)
            xsend[0, 64:128] = (chip[64:128] + rawr[1].astype(F32)).astype(BF16)
            far.append(send(xsend.at[0], xrecv.at[0], to_x))
        elif o == 2:
            up.wait_recv()
            xsend[1, 0:64] = (chip[0:64] + rawr[0].astype(F32)).astype(BF16)
            xsend[1, 64:128] = chip[64:128].astype(BF16)
            far.append(send(xsend.at[1], xrecv.at[1], to_y))
        else:
            own[o] = chip
    for c in far:
        c.wait_recv()
    out[0] = (own[3] + xrecv[0].astype(F32) + xrecv[1].astype(F32)).astype(BF16)
    for c in sent:
        c.wait_send()


N_REMOTE = 150


def body(
    tokens, w_inner, w_gate, w_write, w_read, w_pool_in, w_step, conv_inner, conv_cross, rate_log,
    decay_extra, norm_gain, pool_mix, pool_gain, w_out_inner, w_out_pool,
):
    hbm = pl.BlockSpec(memory_space=pl.ANY)
    V = pltpu.VMEM
    scratch = [
        V((4, 2, T, 512), BF16),
        V((2, 16, 512), BF16),
        V((4, 2, 2, 16, 512), BF16),
        V((8, 8, 16, 256), BF16),
        V((8, 8, 16, 256), BF16),
        V((8, 8, 16, 256), BF16),
        V((8, 8, 16, 128), BF16),
        V((16, 256), BF16),
        V((16, 256), BF16),
        V((16, 128), BF16),
        V((4, 256, 256), BF16),
        V((4, 256, 256), BF16),
        V((4, 2, 8, T), F32),
        V((128, 256), BF16),
        V((2, 16, 1024), BF16),
        V((5, 256), BF16),
        V((5, 2, 128), BF16),
        V((16, 128), F32),
        V((8, 128), F32),
        V((8, 512), F32),
        V((288, 512), F32),
        V((4, 2, 16, 512), F32),
        V((4, T, 256), F32),
        V((4, T, 256), BF16),
        V((4, T, 128), BF16),
        V((4, T, 128), BF16),
        V((4, 8, T), F32),
        V((4, 8, T), F32),
        V((4, T, 128), F32),
        V((4, T, 256), F32),
        V((2, 4, T, 128), BF16),
        V((T, 3 * T), BF16),
        V((4, 2, 128, 256), F32),
        V((8, 256), F32),
        V((8, 256), F32),
        V((2, 4, 2, 32, 256), BF16),
        V((2, 4, 2, 32, 256), BF16),
        V((4, 8, 256), F32),
        V((4, 8, 256), F32),
        V((2, 8, 2, 32, 256), BF16),
        V((8, 8, 256), F32),
        V((8, 256), F32),
        V((2, 4, 2, 32, 256), F32),
        V((2, 2, 32, 256), BF16),
        V((2, 4, 2, 32, 256), BF16),
        V((4, 2, 128, 256), BF16),
        V((4, 128, 1024), F32),
        V((4, 128, 1024), BF16),
        V((4, 128, 1024), BF16),
        V((2, 64, 1024), BF16),
        V((2, 64, 1024), BF16),
        V((2, 128, 1024), BF16),
        V((2, 128, 1024), BF16),
        V((T, 256), BF16),
        V((4, T, 256), BF16),
        pltpu.SemaphoreType.DMA((32,)),
        pltpu.SemaphoreType.DMA((N_REMOTE,)),
        pltpu.SemaphoreType.DMA((N_REMOTE,)),
        pltpu.SemaphoreType.DMA((2, 2)),
    ]
    return pl.pallas_call(
        kernel,
        out_shape=jax.ShapeDtypeStruct((1, 128, 1024), BF16),
        in_specs=[hbm] * 9 + [pl.BlockSpec(memory_space=pltpu.SMEM)] + [hbm] * 6,
        out_specs=pl.BlockSpec(memory_space=pltpu.VMEM),
        scratch_shapes=scratch,
        compiler_params=pltpu.CompilerParams(
            collective_id=0, has_side_effects=True, vmem_limit_bytes=60 * 1024 * 1024
        ),
    )(
        tokens, w_inner, w_gate, w_write, w_read, w_pool_in, jnp.transpose(w_step, (1, 2, 0)),
        conv_inner, conv_cross, rate_log, jnp.transpose(decay_extra[0], (1, 2, 0)),
        norm_gain.reshape(16, 128), pool_mix, pool_gain.reshape(8, 128), w_out_inner, w_out_pool,
    )


def solution(mesh):
    finer = Mesh(
        mesh.devices.reshape(8, 8, mesh.shape["fs"], mesh.shape["tp"]), ("z", "y", "fs", "tp")
    )
    in_specs = (
        P("fs", SP, "tp"),
        P(SP, "tp"),
        P(SP, "tp"),
        P(SP, "tp"),
        P(SP, "tp"),
        P(SP, "tp"),
        P(),
        P(),
        P(),
        P(),
        P("fs", SP, None, "tp"),
        P(),
        P(),
        P(),
        P("tp", "fs"),
        P("tp", "fs"),
    )
    out_specs = P("fs", ("z", "y", "tp"), None)
    return jax.shard_map(body, mesh=finer, in_specs=in_specs, out_specs=out_specs, check_vma=False)
```

time: 96.2 us -> 87.7 us (0.912)
  the two profiles are of different devices: /device:TPU:1 before, /device:TPU:6 now
where the time goes in v3:
time: 87.7 us; the launch traced here: 87.5 us
  Pallas kernels  85.8 us (98%)
  local copies, waits for them, and re-layouts  1.67 us (2%)
    pallas_call x1, Pallas kernels, body(): pl.pallas_call(kernel, out_shape=jax.ShapeDtypeStruct((1, 128, 1024), BF1...  85.8 us

profile of v3, /device:TPU:6, one launch (start us, length us, event | category | flops | bytes accessed | tf_op | source)
XLA Modules:
  0.0 87.5 jit_solution(14714239155079170754)
XLA Ops:
  0.0 85.8 %shard_map.154 = bf16[1,128,1024]{2,1,0:T(8,128)(2,1)} custom-call(bf16[1,256,512]{2,1,0:T(8,128)(2,1)} %tok.1, bf16[16,1024]{1,0:T(8,128)(2,1)} %w_inner.1, bf16[16,1024]{1,0:T(8,128)(2,1)} %w_gate.1, bf16[16,256]{1,0:T(8,128)(2,1)} %w_write.1, bf16[16,256]{1,0:T(8,128)(2,1)} %w_read.1, bf16[16,512]{1,0:T(8,128)(2,1)} %w_pool.1, ...), custom_call_target="tpu_custom_call" | custom-call | tf_op jit(solution)/shard_map/pallas_call | solution.py:618
  85.8 1.7 %copy.18 = bf16[1,128,1024]{2,1,0:T(8,128)(2,1)} copy(bf16[1,128,1024]{2,1,0:T(8,128)(2,1)} %shard_map.154) | data formatting | bytes 524288

commit v4 on v3

--- a/solution.py
+++ b/solution.py
@@ -28,7 +28,7 @@
     tok, w_inner, w_gate, w_write, w_read, w_pool, wst_in, ci_in, cc_in, rate_in, dec_in, ng_in, pmix_in,
     pg_in, woi_in, wop_in,
     out,
-    x_b, hrow, hall, wa1, wa2, wb1, wb2, alt1, alt3, alt4, woi, wop, de, pmix, wst, ci, cc, ng, pg, par,
+    x_b, hrow, hall, wa, wb1, wb2, alt1, alt3, alt4, woi, wop, de, pmix, wst, ci, cc, ng, pg, par,
     p_s, hp, y_s, v_s, b_s, c_s, cum_s, stp_s, cols_s, gate, pool, m_s,
     sb, dec, decp, st, r1, d1, pd, r2, d2, totd, res, tot, inc, b_in, own, dsend, drecv, raws, rawr, xsend, xrecv,
     mix_s, pld_s,
@@ -44,19 +44,44 @@
         v = lax.rem(sp + d, 64)
         return {"z": v // 8, "y": lax.rem(v, 8)}
 
-    count = [0, 0]
+    count = [0, 0, 0]
     sent = []
 
-    def send(src, dst, dev):
-        i = count[0]
-        count[0] += 1
+    def new(kind):
+        count[kind] += 1
+        return count[kind] - 1
+
+    def start(src, dst, dev, si, ri):
         c = pltpu.make_async_remote_copy(
-            src_ref=src, dst_ref=dst, send_sem=ssem.at[i], recv_sem=rsem.at[i],
+            src_ref=src, dst_ref=dst, send_sem=ssem.at[si], recv_sem=rsem.at[ri],
             device_id=dev, device_id_type=MESH,
         )
         c.start()
+        return c
+
+    def all_of(ref, si, ri):
+        return pltpu.make_async_remote_copy(
+            src_ref=ref, dst_ref=ref, send_sem=ssem.at[si], recv_sem=rsem.at[ri],
+            device_id={"tp": 1 - t}, device_id_type=MESH,
+        )
+
+    def send(src, dst, dev):
+        c = start(src, dst, dev, new(0), new(2))
         sent.append(c)
         return c
+
+    def together(items, whole):
+        si, ri = new(0), new(2)
+        for src, dst, dev in items:
+            start(src, dst, dev, si, ri)
+        c = all_of(whole, si, ri)
+        sent.append(c)
+        return c
+
+    def one_send(whole):
+        si = new(0)
+        sent.append(all_of(whole, si, 0))
+        return lambda src, dst, dev: start(src, dst, dev, si, new(2))
 
     def local(src, dst):
         c = pltpu.make_async_copy(src, dst, lsem.at[count[1]])
@@ -94,13 +119,18 @@
     barrier = pltpu.get_barrier_semaphore()
     for p in peers:
         pl.semaphore_signal(barrier, inc=1, device_id=p, device_id_type=MESH)
-    mine1, mine2, mine3, mine4 = (w.at[z, y] for w in (wa1, wa2, wb1, wb2))
+    mine1, mine3, mine4 = (w.at[z, y] for w in (wa, wb1, wb2))
     tok_local = local(tok.at[0], x_b.at[r, t])
     w_local = [
-        local(w_inner.at[:, at(r, 256)], mine1),
-        local(w_inner.at[:, at(r_y, 256)], alt1),
-        local(w_write.at[:, at(fq, 128)], mine2.at[:, pl.ds(0, 128)]),
-        local(w_read.at[:, at(fq, 128)], mine2.at[:, pl.ds(128, 128)]),
+        local(w_inner.at[:, at(q, 256)], m.at[:, pl.ds(0, 256)])
+        for q, m in ((r, mine1), (r_y, alt1))
+    ]
+    w_local += [
+        local(w.at[:, at(fq, 128)], m.at[:, pl.ds(c, 128)])
+        for w, c in ((w_write, 256), (w_read, 384))
+        for m in (mine1, alt1)
+    ]
+    w_local += [
         local(w_gate.at[:, at(r, 256)], mine3),
         local(w_gate.at[:, at(r_y, 256)], alt3),
         local(w_pool.at[:, at(r, 128)], mine4),
@@ -123,86 +153,85 @@
     pl.semaphore_wait(barrier, len(peers))
 
     x_own = x_b.at[r, t]
-    edge_n = send(x_own.at[pl.ds(240, 16)], hrow.at[0], along(1))
-    edge_p = send(x_own.at[pl.ds(0, 16)], hrow.at[1], along(63))
-
-    def stage(mine, alt):
-        return [send(alt if d % 2 else mine, mine, {"y": ymod(d)}) for d in near_first]
-
-    first, second = stage(mine1, alt1), stage(mine2, mine2)
-    x_right = send(x_own, x_own, to_x)
-    x_left = send(x_own, x_own, to_y)
-    x_pair = [send(x_own, x_own, pair)]
-    decs = [
-        send(dec_in.at[:, at(q, 8)], de.at[r], g)
-        for q, g in ((1 - fq, to_x), (fq, to_y), (1 - fq, to_d))
-    ]
-    third, fourth = stage(mine3, alt3), stage(mine4, alt4)
-
-    def ring_z(w, k, to):
-        s = w.at[zmod(8 - k if to == 1 else k)]
-        if k == 3:
-            s = s.at[pl.ds(0 if to == 1 else 4, 4)]
-        return send(s, s, {"z": zmod(to)})
+    edges = together(
+        [
+            (x_own.at[pl.ds(240, 16)], hrow.at[0], along(1)),
+            (x_own.at[pl.ds(0, 16)], hrow.at[1], along(63)),
+        ],
+        hrow,
+    )
+
+    def stage(w, mine, alt):
+        items = [(alt if d % 2 else mine, mine, {"y": ymod(d)}) for d in near_first]
+        return together(items, w.at[0, pl.ds(0, 7)])
+
+    first = stage(wa, mine1, alt1)
+    send_x = one_send(x_b.at[pl.ds(0, 2), 0])
+    x_right = send_x(x_own, x_own, to_x)
+    x_left = send_x(x_own, x_own, to_y)
+    pair_i = (new(0), new(2))
+
+    def to_pair(block):
+        start(block, block, pair, *pair_i)
+
+    x_pair = all_of(x_b.at[pl.ds(0, 3), 0], *pair_i)
+    sent.append(x_pair)
+    to_pair(x_own)
+    decs = together(
+        [
+            (dec_in.at[:, at(q, 8)], de.at[r], g)
+            for q, g in ((1 - fq, to_x), (fq, to_y), (1 - fq, to_d))
+        ],
+        de.at[pl.ds(0, 3)],
+    )
 
     rings = {}
 
-    def begin(name, w):
-        rings[name] = [(w, to, [ring_z(w, 0, to)]) for to in (1, 7)]
+    def hop(piece, k, to):
+        (w, a, n, only), issue = piece
+        if k == 3 and only is None:
+            a, n = (a if to == 1 else a + n // 2), n // 2
+        s = w.at[zmod(8 - k if to == 1 else k), pl.ds(a, n)]
+        return issue(s, s, {"z": zmod(to)})
+
+    def begin(name, w, halves):
+        pieces = [(w, i, 2, 1 if i < 4 else 7) for i in range(0, 8, 2)] if halves else [(w, 0, 8, None)]
+        issue = one_send(w.at[pl.ds(0, 7)])
+        rings[name] = [((p, issue), to, [hop((p, issue), 0, to)]) for p in pieces for to in (1, 7)]
 
     def step(names, k):
         for name in names:
-            for w, to, ring in rings[name]:
-                ring[k - 1].wait_recv()
-                if k < 4:
-                    ring.append(ring_z(w, k, to))
-
-    for c in first:
-        c.wait_recv()
-    begin("a1", wa1)
-    for c in second:
-        c.wait_recv()
-    begin("a2", wa2)
-    edge_n.wait_recv()
-    edge_p.wait_recv()
-    halo_local = local(hrow, hall.at[r, t])
-    halos = [send(hrow, hall.at[r, t], g) for g in group]
-    step(("a1", "a2"), 1)
+            for piece, to, ring in rings[name]:
+                last = piece[0][3] is not None and piece[0][3] != to
+                if k < 4 or not last:
+                    ring[k - 1].wait_recv()
+                if k < 3 or (k == 3 and not last):
+                    ring.append(hop(piece, k, to))
+
+    first.wait_recv()
+    begin("a", wa, True)
+    edges.wait_recv()
+    halo_local = local(hrow, hall.at[r * 2 + t])
+    halos = together([(hrow, hall.at[r * 2 + t], g) for g in group], hall.at[pl.ds(0, 7)])
+    step(("a",), 1)
     x_right.wait_recv()
     block = x_b.at[r_x, t]
-    x_fr = send(block.at[pl.ds(0, 128)], block.at[pl.ds(0, 128)], to_y)
-    x_pair.append(send(block, block, pair))
+    far_i = (new(0), new(2))
+    x_far = all_of(x_b.at[r_d, t], *far_i)
+    sent.append(x_far)
+    start(block.at[pl.ds(0, 64)], block.at[pl.ds(0, 64)], to_y, *far_i)
+    to_pair(block)
     x_left.wait_recv()
     block = x_b.at[r_y, t]
-    x_fl = send(block.at[pl.ds(128, 128)], block.at[pl.ds(128, 128)], to_x)
-    x_pair.append(send(block, block, pair))
-    step(("a1", "a2"), 2)
+    start(block.at[pl.ds(64, 192)], block.at[pl.ds(64, 192)], to_x, *far_i)
+    to_pair(block)
+    fourth, third = stage(wb2, mine4, alt4), stage(wb1, mine3, alt3)
+    step(("a",), 2)
     for c in others:
         c.wait()
     par[0:5, 0:256] = ci[...].astype(F32)
     par[0:5, 256:384] = cc[:, 0, :].astype(F32)
     par[0:5, 384:512] = cc[:, 1, :].astype(F32)
-    x_fr.wait_recv()
-    x_fl.wait_recv()
-    block = x_b.at[r_d, t]
-    x_pair.append(send(block, block, pair))
-    step(("a1", "a2"), 3)
-    for c in third + fourth:
-        c.wait_recv()
-    begin("b1", wb1)
-    begin("b2", wb2)
-    wos = []
-    for d in (1, 3, 2):
-        g = fmod(d)
-        q = lax.rem(g, 2)
-        wos.append(send(woi_in.at[at(q * 2 + yq, 256)], woi.at[f], {"fs": g}))
-        wos.append(send(wop_in.at[at(q, 256)], wop.at[f], {"fs": g}))
-
-    def gate_step(k):
-        step(("b1", "b2"), k)
-
-    for c in x_pair + decs:
-        c.wait_recv()
     ii = lax.broadcasted_iota(jnp.int32, (T, T), 0)
     jj = lax.broadcasted_iota(jnp.int32, (T, T), 1)
     low = lax.broadcasted_iota(jnp.int32, (T, 128), 1) < 64
@@ -218,14 +247,14 @@
     for i in range(8):
         rate = jnp.where(r8 == i, rate_in[i // 4, t * 16 + r * 4 + i % 4], rate)
     rate = jnp.exp(rate)
+
     def pick(rows, which, n):
         chosen = rows[0:4]
         for i in range(1, n):
             chosen = jnp.where(which == i, rows[4 * i : 4 * i + 4], chosen)
         return chosen
 
-    lds = []
-    for o in range(4):
+    def decay_rows(o):
         s = slot_unit(o)
         w0, w1 = wst[:, :, 0:512].reshape(32, 512), wst[:, :, 512:1024].reshape(32, 512)
         all_raw = dot(w0, x_b[s, 0], ((1,), (1,))) + dot(w1, x_b[s, 1], ((1,), (1,)))
@@ -233,8 +262,33 @@
         extra = jnp.concatenate([pick(de[s, 0], yq, 2), pick(de[s, 1], yq, 2)], axis=0)
         stp = jnp.maximum(raw, 0.0) + jnp.log1p(jnp.exp(-jnp.abs(raw)))
         stp_s[o] = stp
-        lds.append(extra - stp * rate)
-    ld = jnp.concatenate(lds, axis=0)
+        cum_s[o] = extra - stp * rate
+
+    x_pair.wait_recv()
+    decs.wait_recv()
+    for o in (3, 2, 1):
+        decay_rows(o)
+    step(("a",), 3)
+    x_far.wait_recv()
+    block = x_b.at[r_d, t]
+    far_pair = send(block, block, pair)
+    fourth.wait_recv()
+    begin("b2", wb2, False)
+    third.wait_recv()
+    begin("b1", wb1, False)
+    dests = [(fmod(d), lax.rem(fmod(d), 2)) for d in (1, 3, 2)]
+    wos = [
+        together(
+            [(woi_in.at[at(q * 2 + yq, 256)], woi.at[f], {"fs": g}) for g, q in dests],
+            woi.at[pl.ds(0, 3)],
+        ),
+        together(
+            [(wop_in.at[at(q, 256)], wop.at[f], {"fs": g}) for g, q in dests], wop.at[pl.ds(0, 3)]
+        ),
+    ]
+    far_pair.wait_recv()
+    decay_rows(0)
+    ld = cum_s[...].reshape(32, T)
     ld_a = ld.astype(BF16)
     rest = ld - ld_a.astype(F32)
     ld_b = rest.astype(BF16)
@@ -261,27 +315,27 @@
     both = [ends[4 * hf + n] + ends[4 * hf + 2 + n] for hf in range(2) for n in range(2)]
     decp[...] = jnp.concatenate(both + [jnp.zeros((4, 256), F32)], axis=0)
     own_dec = local(decp, d1.at[yp])
-    sd1 = [send(decp, d1.at[yp], {"y": ymod(2 * d)}) for d in (1, 3, 2)]
+    sd1 = together([(decp, d1.at[yp], {"y": ymod(2 * d)}) for d in (1, 3, 2)], d1.at[pl.ds(0, 3)])
 
     halo_local.wait()
-    for c in halos:
-        c.wait_recv()
-    step(("a1", "a2"), 4)
+    halos.wait_recv()
+    step(("a",), 4)
+    step(("b2",), 1)
 
     def rows_of(w, k, n):
         return w[4 * k : 4 * k + 4].reshape(512, n)
 
-    h0 = hall[:, 0].reshape(128, 512)
-    h1 = hall[:, 1].reshape(128, 512)
-    hrow_at = lax.broadcasted_iota(jnp.int32, (128, 256), 0)
+    halls = hall[...].reshape(4, 2, 2, 16, 512)
+    h0 = halls[:, 0].reshape(128, 512)
+    h1 = halls[:, 1].reshape(128, 512)
+    hrow_at = lax.broadcasted_iota(jnp.int32, (128, 512), 0)
     side = lax.rem(hrow_at // 16, 2)
     place = sp - yq + lax.rem(hrow_at // 32, 2)
     gone = jnp.logical_or(
         jnp.logical_and(side == 0, place == 0), jnp.logical_and(side == 1, place == 63)
     )
-    for i, w in enumerate((wa1, wa2)):
-        hproj = (dot(h0, rows_of(w, 0, 256)) + dot(h1, rows_of(w, 1, 256))).astype(BF16).astype(F32)
-        hp[:, :, :, i * 256 : (i + 1) * 256] = jnp.where(gone, 0.0, hproj).reshape(4, 2, 16, 256)
+    hproj = (dot(h0, rows_of(wa, 0, 512)) + dot(h1, rows_of(wa, 1, 512))).astype(BF16).astype(F32)
+    hp[...] = jnp.where(gone, 0.0, hproj).reshape(4, 2, 16, 512)
 
     def spread(cols, c):
         parts = [
@@ -293,9 +347,8 @@
     def front(o):
         s = slot_unit(o)
         x0, x1 = x_b[s, 0], x_b[s, 1]
-        for i, w in enumerate((wa1, wa2)):
-            pa = dot(x0, rows_of(w, 0, 256)) + dot(x1, rows_of(w, 1, 256))
-            p_s[16:272, i * 256 : (i + 1) * 256] = pa.astype(BF16).astype(F32)
+        pa = dot(x0, rows_of(wa, 0, 512)) + dot(x1, rows_of(wa, 1, 512))
+        p_s[16:272, :] = pa.astype(BF16).astype(F32)
         p_s[0:16, :] = hp[s, 0]
         p_s[272:288, :] = hp[s, 1]
         conv = p_s[14 : 14 + T, :] * par[0:1, :]
@@ -348,12 +401,13 @@
         lax.fori_loop(2 * hf, 2 * hf + 2, front_step, 0)
         join(hf)
         own_st.append(local(st.at[hf, yp], r1.at[hf, yp]))
-        s1.append([send(st.at[hf, pmod(d)], r1.at[hf, yp], {"y": ymod(2 * d)}) for d in (1, 3, 2)])
-        gate_step(hf + 1)
+        items = [(st.at[hf, pmod(d)], r1.at[hf, yp], {"y": ymod(2 * d)}) for d in (1, 3, 2)]
+        s1.append(together(items, r1.at[hf, pl.ds(0, 3)]))
+        step(("b2",), hf + 2)
+        step(("b1",), hf + 1)
         if hf == 0:
             own_dec.wait()
-            for c in sd1:
-                c.wait_recv()
+            sd1.wait_recv()
             cumf = jnp.zeros((8, 256), F32)
             cumb = jnp.zeros((8, 256), F32)
             back = lax.rem(lax.broadcasted_iota(jnp.int32, (8, 256), 0), 2) == 1
@@ -365,7 +419,8 @@
                 pd[i] = jnp.exp(jnp.where(back, cumb, pf[i]))
                 cumb = cumb + d1[i]
             totd[...] = cumf
-            sd2 = [send(totd, d2.at[z], {"z": zmod(d)}) for d in near_first]
+            items = [(totd, d2.at[z], {"z": zmod(d)}) for d in near_first]
+            sd2 = together(items, d2.at[pl.ds(0, 7)])
 
     def inner(o, _):
         cols, cu, stp = cols_s[o], cum_s[o], stp_s[o]
@@ -388,8 +443,7 @@
 
     def scan1(hf):
         own_st[hf].wait()
-        for c in s1[hf]:
-            c.wait_recv()
+        s1[hf].wait_recv()
         for n in range(2):
             run = jnp.zeros((32, 256), F32)
             for i in range(4) if n == 0 else reversed(range(4)):
@@ -397,14 +451,14 @@
                 w = jnp.exp(d1[i, 2 * hf + n : 2 * hf + n + 1, :])
                 run = run * w + r1[hf, i, n].astype(F32)
             tot[hf, n] = run.astype(BF16)
-        return [
-            send(tot.at[hf, (z + d) // 8], r2.at[hf, z, (z + d) // 8], {"z": zmod(d)})
+        items = [
+            (tot.at[hf, (z + d) // 8], r2.at[hf, z, (z + d) // 8], {"z": zmod(d)})
             for d in near_first
         ]
+        return together(items, r2.at[hf, pl.ds(0, 7), 0])
 
     def scan2(hf, s2):
-        for c in s2:
-            c.wait_recv()
+        s2.wait_recv()
         for n in range(2):
             acc = jnp.zeros((32, 256), F32)
             for i in range(8) if n == 0 else reversed(range(8)):
@@ -416,16 +470,18 @@
                 w = pd[i, 2 * hf + n : 2 * hf + n + 1, :]
                 r1[hf, i, n] = (res[hf, i, n] + acc * w).astype(BF16)
         mine = local(r1.at[hf, yp], inc.at[hf, yp])
-        return mine, [
-            send(r1.at[hf, pmod(d)], inc.at[hf, yp], {"y": ymod(2 * d)}) for d in (1, 3, 2)
-        ]
+        items = [(r1.at[hf, pmod(d)], inc.at[hf, yp], {"y": ymod(2 * d)}) for d in (1, 3, 2)]
+        return mine, together(items, inc.at[hf, pl.ds(0, 3)])
 
     def gates(o, _):
         s = slot_unit(o)
-        x0, x1 = x_b[s, 0], x_b[s, 1]
-        g = dot(x0, rows_of(wb1, 0, 256)) + dot(x1, rows_of(wb1, 1, 256))
+        g = dot(x_b[s, 0], rows_of(wb1, 0, 256)) + dot(x_b[s, 1], rows_of(wb1, 1, 256))
         gate[o] = silu(g.astype(BF16).astype(F32))
-        q = dot(x0, rows_of(wb2, 0, 128)) + dot(x1, rows_of(wb2, 1, 128))
+        return _
+
+    def grids(o, _):
+        s = slot_unit(o)
+        q = dot(x_b[s, 0], rows_of(wb2, 0, 128)) + dot(x_b[s, 1], rows_of(wb2, 1, 128))
         pool[o // 2, 1 + slot_block(o)] = q.astype(BF16)
         return _
 
@@ -441,24 +497,6 @@
         ]
 
     lax.fori_loop(0, 2, inner, 0)
-    gate_step(3)
-    s2_0 = scan1(0)
-    lax.fori_loop(2, 4, inner, 0)
-    gate_step(4)
-    s2_1 = scan1(1)
-    for c in sd2:
-        c.wait_recv()
-    s3_0 = scan2(0, s2_0)
-    lax.fori_loop(0, 4, gates, 0)
-    for g in range(4):
-
-        @pl.when(group_at == g)
-        def _():
-            for c in pool_copies(g):
-                c.start()
-
-    s3_1 = scan2(1, s2_1)
-
     k = jnp.left_shift(jnp.int32(2), group_at)
     ti = lax.broadcasted_iota(jnp.int32, (T, 3 * T), 0)
     tj = lax.broadcasted_iota(jnp.int32, (T, 3 * T), 1)
@@ -466,6 +504,25 @@
     rj, cj = tj // GRID_W, lax.rem(tj, GRID_W)
     inside = (rj >= ri - k // 2) & (rj < ri + k // 2) & (cj >= ci_ - k // 2) & (cj < ci_ + k // 2)
     m_s[...] = inside.astype(F32).astype(BF16)
+    s2_0 = scan1(0)
+    step(("b2",), 4)
+    lax.fori_loop(0, 4, grids, 0)
+    for g in range(4):
+
+        @pl.when(group_at == g)
+        def _():
+            for c in pool_copies(g):
+                c.start()
+
+    step(("b1",), 3)
+    lax.fori_loop(2, 4, inner, 0)
+    s2_1 = scan1(1)
+    sd2.wait_recv()
+    s3_0 = scan2(0, s2_0)
+    step(("b1",), 4)
+    lax.fori_loop(0, 4, gates, 0)
+    s3_1 = scan2(1, s2_1)
+
     for g in range(4):
 
         @pl.when(group_at == g)
@@ -503,49 +560,71 @@
 
     mine = at(t, 128)
     theirs = at(1 - t, 128)
-    far = []
-    for o in range(4):
-        if o % 2 == 0:
-            s3 = s3_0 if o == 0 else s3_1
-            s3[0].wait()
-            for c in s3[1]:
-                c.wait_recv()
-            enter(o // 2)
+    swaps = []
+    swap_send = one_send(dsend)
+    raw_send = one_send(raws)
+    out_i = (new(0), new(2))
+    far = all_of(xrecv, *out_i)
+    sent.append(far)
+
+    def produce(o):
         finish(o)
         for q in range(4):
             cs = slice(q * 256, (q + 1) * 256)
             part = dot(mix_s[theirs, :], woi[q]) + dot(pld_s[o, theirs, :], wop[q])
             dsend[o, :, cs] = part.astype(BF16)
-        swap = send(dsend.at[o], drecv.at[o], pair)
+        swaps.append(swap_send(dsend.at[o], drecv.at[o], pair))
         for q in range(4):
             cs = slice(q * 256, (q + 1) * 256)
             own[o, :, cs] = dot(mix_s[mine, :], woi[q]) + dot(pld_s[o, mine, :], wop[q])
-        swap.wait_recv()
-        chip = own[o] + drecv[o].astype(F32)
-        if o == 0:
-            raws[...] = chip.astype(BF16).reshape(2, 64, 1024)
-            up = send(raws.at[0], rawr.at[0], to_x)
-            down = send(raws.at[1], rawr.at[1], to_y)
-        elif o == 1:
-            down.wait_recv()
-            xsend[0, 0:64] = chip[0:64].astype(BF16)
-            xsend[0, 64:128] = (chip[64:128] + rawr[1].astype(F32)).astype(BF16)
-            far.append(send(xsend.at[0], xrecv.at[0], to_x))
-        elif o == 2:
-            up.wait_recv()
-            xsend[1, 0:64] = (chip[0:64] + rawr[0].astype(F32)).astype(BF16)
-            xsend[1, 64:128] = chip[64:128].astype(BF16)
-            far.append(send(xsend.at[1], xrecv.at[1], to_y))
-        else:
-            own[o] = chip
-    for c in far:
-        c.wait_recv()
-    out[0] = (own[3] + xrecv[0].astype(F32) + xrecv[1].astype(F32)).astype(BF16)
+
+    def chip_sum(o):
+        swaps[o].wait_recv()
+        return (own[o] + drecv[o].astype(F32)).reshape(2, 64, 1024)
+
+    def arrive(hf, s3):
+        s3[0].wait()
+        s3[1].wait_recv()
+        enter(hf)
+
+    def out_half(i, h, value, dev, a=0):
+        n = value.shape[0]
+        xsend[i, h, a : a + n] = value.astype(BF16)
+        rows = pl.ds(a, n)
+        start(xsend.at[i, h, rows], xrecv.at[i, h, rows], dev, *out_i)
+
+    arrive(0, s3_0)
+    produce(0)
+    produce(1)
+    raws[...] = chip_sum(0).astype(BF16)
+    up, down = [], []
+    for q in range(2):
+        rows = pl.ds(q * 32, 32)
+        up.append(raw_send(raws.at[0, rows], rawr.at[0, rows], to_x))
+        down.append(raw_send(raws.at[1, rows], rawr.at[1, rows], to_y))
+    chip1 = chip_sum(1)
+    out_half(0, 0, chip1[0], to_x)
+    own[1, 64:128] = chip1[1]
+    arrive(1, s3_1)
+    produce(2)
+    produce(3)
+    chip2 = chip_sum(2)
+    out_half(1, 1, chip2[1], to_y)
+    for q in range(2):
+        a = q * 32
+        down[q].wait_recv()
+        out_half(0, 1, own[1, 64 + a : 96 + a] + rawr[1, a : a + 32].astype(F32), to_x, a)
+        up[q].wait_recv()
+        out_half(1, 0, chip2[0, a : a + 32] + rawr[0, a : a + 32].astype(F32), to_y, a)
+    own[3] = chip_sum(3).reshape(128, 1024)
+    far.wait_recv()
+    arrived = (xrecv[0].astype(F32) + xrecv[1].astype(F32)).reshape(128, 1024)
+    out[0] = (own[3] + arrived).astype(BF16)
     for c in sent:
         c.wait_send()
 
 
-N_REMOTE = 150
+N_LOCAL, N_SEND, N_RECV = 26, 26, 74
 
 
 def body(
@@ -557,12 +636,11 @@
     scratch = [
         V((4, 2, T, 512), BF16),
         V((2, 16, 512), BF16),
-        V((4, 2, 2, 16, 512), BF16),
-        V((8, 8, 16, 256), BF16),
-        V((8, 8, 16, 256), BF16),
+        V((8, 2, 16, 512), BF16),
+        V((8, 8, 16, 512), BF16),
         V((8, 8, 16, 256), BF16),
         V((8, 8, 16, 128), BF16),
-        V((16, 256), BF16),
+        V((16, 512), BF16),
         V((16, 256), BF16),
         V((16, 128), BF16),
         V((4, 256, 256), BF16),
@@ -606,13 +684,13 @@
         V((4, 128, 1024), BF16),
         V((2, 64, 1024), BF16),
         V((2, 64, 1024), BF16),
-        V((2, 128, 1024), BF16),
-        V((2, 128, 1024), BF16),
+        V((2, 2, 64, 1024), BF16),
+        V((2, 2, 64, 1024), BF16),
         V((T, 256), BF16),
         V((4, T, 256), BF16),
-        pltpu.SemaphoreType.DMA((32,)),
-        pltpu.SemaphoreType.DMA((N_REMOTE,)),
-        pltpu.SemaphoreType.DMA((N_REMOTE,)),
+        pltpu.SemaphoreType.DMA((N_LOCAL,)),
+        pltpu.SemaphoreType.DMA((N_SEND,)),
+        pltpu.SemaphoreType.DMA((N_RECV,)),
         pltpu.SemaphoreType.DMA((2, 2)),
     ]
     return pl.pallas_call(

time: 87.7 us -> 78.4 us (0.89)
  the two profiles are of different devices: /device:TPU:6 before, /device:TPU:1 now
where the time goes in v4:
time: 78.4 us; the launch traced here: 77.7 us
  Pallas kernels  76 us (97%)
  local copies, waits for them, and re-layouts  1.67 us (2%)
    pallas_call x1, Pallas kernels, body(): pl.pallas_call(kernel, out_shape=jax.ShapeDtypeStruct((1, 128, 1024), BF1...  76 us
    unnamed x1, local copies, waits for them, and re-layouts  1.67 us

profile of v4, /device:TPU:1, one launch (start us, length us, event | category | flops | bytes accessed | tf_op | source)
XLA Modules:
  0.0 77.7 jit_solution(11079520998909271759)
XLA Ops:
  0.0 76.0 %shard_map.154 = bf16[1,128,1024]{2,1,0:T(8,128)(2,1)} custom-call(bf16[1,256,512]{2,1,0:T(8,128)(2,1)} %tok.1, bf16[16,1024]{1,0:T(8,128)(2,1)} %w_inner.1, bf16[16,1024]{1,0:T(8,128)(2,1)} %w_gate.1, bf16[16,256]{1,0:T(8,128)(2,1)} %w_write.1, bf16[16,256]{1,0:T(8,128)(2,1)} %w_read.1, bf16[16,512]{1,0:T(8,128)(2,1)} %w_pool.1, ...), custom_call_target="tpu_custom_call" | custom-call | tf_op jit(solution)/shard_map/pallas_call | solution.py:696
  76.0 1.7 %copy.18 = bf16[1,128,1024]{2,1,0:T(8,128)(2,1)} copy(bf16[1,128,1024]{2,1,0:T(8,128)(2,1)} %shard_map.154) | data formatting | bytes 524288

commit v5 on v4

--- a/solution.py
+++ b/solution.py
@@ -28,8 +28,8 @@
     tok, w_inner, w_gate, w_write, w_read, w_pool, wst_in, ci_in, cc_in, rate_in, dec_in, ng_in, pmix_in,
     pg_in, woi_in, wop_in,
     out,
-    x_b, hrow, hall, wa, wb1, wb2, alt1, alt3, alt4, woi, wop, de, pmix, wst, ci, cc, ng, pg, par,
-    p_s, hp, y_s, v_s, b_s, c_s, cum_s, stp_s, cols_s, gate, pool, m_s,
+    x_b, hrow, hall, wa, wb1, wb2, alt1, alt3, alt4, woi, wop, de, pmix, wst, rate_s, ci, cc, ng, pg, par,
+    p_s, p_r, hp, y_s, v_s, b_s, c_s, cum_s, stp_s, cols_s, gate, pool, m_s,
     sb, dec, decp, st, r1, d1, pd, r2, d2, totd, res, tot, inc, b_in, own, dsend, drecv, raws, rawr, xsend, xrecv,
     mix_s, pld_s,
     lsem, ssem, rsem, psem,
@@ -114,8 +114,6 @@
     peers = [{"y": ymod(d)} for d in range(1, 8)] + [{"z": zmod(d)} for d in range(1, 8)]
     peers += group + [{"fs": fmod(d)} for d in range(1, 4)] + [along(d) for d in (1, 63, 2, 62)]
 
-    pool[:, 0] = jnp.zeros((2, T, 128), BF16)
-    pool[:, 3] = jnp.zeros((2, T, 128), BF16)
     barrier = pltpu.get_barrier_semaphore()
     for p in peers:
         pl.semaphore_signal(barrier, inc=1, device_id=p, device_id_type=MESH)
@@ -142,11 +140,14 @@
         local(ci_in.at[:, at(t * 4 + r, 256)], ci),
         local(cc_in.at[:, :, at(group_at, 128)], cc),
         local(ng_in, ng),
+        local(rate_in, rate_s),
         local(pg_in, pg),
         local(pmix_in.at[group_at, at(yq, 128)], pmix),
         local(woi_in.at[at(r, 256)], woi.at[f]),
         local(wop_in.at[at(fq, 256)], wop.at[f]),
     ]
+    pool[:, 0] = jnp.zeros((2, T, 128), BF16)
+    pool[:, 3] = jnp.zeros((2, T, 128), BF16)
     tok_local.wait()
     for c in w_local:
         c.wait()
@@ -245,7 +246,7 @@
     r8 = lax.broadcasted_iota(jnp.int32, (8, 1), 0)
     rate = jnp.zeros((8, 1), F32)
     for i in range(8):
-        rate = jnp.where(r8 == i, rate_in[i // 4, t * 16 + r * 4 + i % 4], rate)
+        rate = jnp.where(r8 == i, rate_s[i // 4, t * 16 + r * 4 + i % 4], rate)
     rate = jnp.exp(rate)
 
     def pick(rows, which, n):
@@ -344,23 +345,26 @@
         ]
         return jnp.concatenate(parts, axis=1)
 
+    def convolve(s, x0, x1, buf, c, n):
+        cs = slice(c, c + n)
+        w0, w1 = (wa[4 * k : 4 * k + 4, :, :, cs].reshape(512, n) for k in range(2))
+        buf[16:272, :] = (dot(x0, w0) + dot(x1, w1)).astype(BF16).astype(F32)
+        buf[0:16, :] = hp[s, 0, :, cs]
+        buf[272:288, :] = hp[s, 1, :, cs]
+        conv = buf[14 : 14 + T, :] * par[0:1, cs]
+        for j in range(1, 5):
+            conv = conv + buf[14 + j : 14 + j + T, :] * par[j : j + 1, cs]
+        return silu(conv)
+
     def front(o):
         s = slot_unit(o)
         x0, x1 = x_b[s, 0], x_b[s, 1]
-        pa = dot(x0, rows_of(wa, 0, 512)) + dot(x1, rows_of(wa, 1, 512))
-        p_s[16:272, :] = pa.astype(BF16).astype(F32)
-        p_s[0:16, :] = hp[s, 0]
-        p_s[272:288, :] = hp[s, 1]
-        conv = p_s[14 : 14 + T, :] * par[0:1, :]
-        for j in range(1, 5):
-            conv = conv + p_s[14 + j : 14 + j + T, :] * par[j : j + 1, :]
-        act = silu(conv)
-        v, b, c = act[:, 0:256], act[:, 256:384], act[:, 384:512]
+        act = convolve(s, x0, x1, p_s, 0, 384)
+        v, b = act[:, 0:256], act[:, 256:384]
         cols = jnp.concatenate([cum_s[o], stp_s[o], jnp.zeros((112, T), F32)], axis=0).T
         cols_s[o] = cols
         v_s[o] = v.astype(BF16)
         b_s[o] = b.astype(BF16)
-        c_s[o] = c.astype(BF16)
         bt = b.T.astype(BF16)
         lane = lax.broadcasted_iota(jnp.int32, (1, 128), 1)
         end = jnp.where(lane < 4, cols[T - 1 : T, :], cols[0:1, :])
@@ -423,6 +427,8 @@
             sd2 = together(items, d2.at[pl.ds(0, 7)])
 
     def inner(o, _):
+        s = slot_unit(o)
+        c_s[o] = convolve(s, x_b[s, 0], x_b[s, 1], p_r, 384, 128).astype(BF16)
         cols, cu, stp = cols_s[o], cum_s[o], stp_s[o]
         scores = dot(c_s[o], b_s[o], ((1,), (1,)))
         for q in range(2):
@@ -521,8 +527,6 @@
     s3_0 = scan2(0, s2_0)
     step(("b1",), 4)
     lax.fori_loop(0, 4, gates, 0)
-    s3_1 = scan2(1, s2_1)
-
     for g in range(4):
 
         @pl.when(group_at == g)
@@ -546,6 +550,8 @@
         return _
 
     lax.fori_loop(0, 4, pools, 0)
+
+    s3_1 = scan2(1, s2_1)
 
     for c in wos:
         c.wait_recv()
@@ -624,7 +630,7 @@
         c.wait_send()
 
 
-N_LOCAL, N_SEND, N_RECV = 26, 26, 74
+N_LOCAL, N_SEND, N_RECV = 27, 26, 74
 
 
 def body(
@@ -648,12 +654,14 @@
         V((4, 2, 8, T), F32),
         V((128, 256), BF16),
         V((2, 16, 1024), BF16),
+        pltpu.SMEM((2, 32), F32),
         V((5, 256), BF16),
         V((5, 2, 128), BF16),
         V((16, 128), F32),
         V((8, 128), F32),
         V((8, 512), F32),
-        V((288, 512), F32),
+        V((288, 384), F32),
+        V((288, 128), F32),
         V((4, 2, 16, 512), F32),
         V((4, T, 256), F32),
         V((4, T, 256), BF16),
@@ -696,7 +704,7 @@
     return pl.pallas_call(
         kernel,
         out_shape=jax.ShapeDtypeStruct((1, 128, 1024), BF16),
-        in_specs=[hbm] * 9 + [pl.BlockSpec(memory_space=pltpu.SMEM)] + [hbm] * 6,
+        in_specs=[hbm] * 16,
         out_specs=pl.BlockSpec(memory_space=pltpu.VMEM),
         scratch_shapes=scratch,
         compiler_params=pltpu.CompilerParams(

time: 78.4 us -> 76.8 us (0.980)
  Pallas kernels: 76 us -> 75 us
    pallas_call x1, Pallas kernels: 76 us -> 75 us  [body(): pl.pallas_call(kernel, out_shape=jax.ShapeDtypeStruct((1, 128, 1024), BF1...]
where the time goes in v5:
time: 76.8 us; the launch traced here: 76.7 us
  Pallas kernels  75 us (98%)
  local copies, waits for them, and re-layouts  1.67 us (2%)
    pallas_call x1, Pallas kernels, body(): pl.pallas_call(kernel, out_shape=jax.ShapeDtypeStruct((1, 128, 1024), BF1...  75 us
    unnamed x1, local copies, waits for them, and re-layouts  1.67 us

profile of v5, /device:TPU:1, one launch (start us, length us, event | category | flops | bytes accessed | tf_op | source)
XLA Modules:
  0.0 76.7 jit_solution(8018566541812770581)
XLA Ops:
  0.0 75.0 %shard_map.154 = bf16[1,128,1024]{2,1,0:T(8,128)(2,1)} custom-call(bf16[1,256,512]{2,1,0:T(8,128)(2,1)} %tok.1, bf16[16,1024]{1,0:T(8,128)(2,1)} %w_inner.1, bf16[16,1024]{1,0:T(8,128)(2,1)} %w_gate.1, bf16[16,256]{1,0:T(8,128)(2,1)} %w_write.1, bf16[16,256]{1,0:T(8,128)(2,1)} %w_read.1, bf16[16,512]{1,0:T(8,128)(2,1)} %w_pool.1, ...), custom_call_target="tpu_custom_call" | custom-call | tf_op jit(solution)/shard_map/pallas_call | solution.py:704
  75.0 1.7 %copy.18 = bf16[1,128,1024]{2,1,0:T(8,128)(2,1)} copy(bf16[1,128,1024]{2,1,0:T(8,128)(2,1)} %shard_map.154) | data formatting | bytes 524288

commit v6 on v5

--- a/solution.py
+++ b/solution.py
@@ -154,6 +154,11 @@
     pl.semaphore_wait(barrier, len(peers))
 
     x_own = x_b.at[r, t]
+    def stage(w, mine, alt):
+        items = [(alt if d % 2 else mine, mine, {"y": ymod(d)}) for d in near_first]
+        return together(items, w.at[0, pl.ds(0, 7)])
+
+    first = stage(wa, mine1, alt1)
     edges = together(
         [
             (x_own.at[pl.ds(240, 16)], hrow.at[0], along(1)),
@@ -161,12 +166,6 @@
         ],
         hrow,
     )
-
-    def stage(w, mine, alt):
-        items = [(alt if d % 2 else mine, mine, {"y": ymod(d)}) for d in near_first]
-        return together(items, w.at[0, pl.ds(0, 7)])
-
-    first = stage(wa, mine1, alt1)
     send_x = one_send(x_b.at[pl.ds(0, 2), 0])
     x_right = send_x(x_own, x_own, to_x)
     x_left = send_x(x_own, x_own, to_y)
@@ -521,8 +520,8 @@
                 c.start()
 
     step(("b1",), 3)
+    s2_1 = scan1(1)
     lax.fori_loop(2, 4, inner, 0)
-    s2_1 = scan1(1)
     sd2.wait_recv()
     s3_0 = scan2(0, s2_0)
     step(("b1",), 4)
@@ -608,11 +607,11 @@
         rows = pl.ds(q * 32, 32)
         up.append(raw_send(raws.at[0, rows], rawr.at[0, rows], to_x))
         down.append(raw_send(raws.at[1, rows], rawr.at[1, rows], to_y))
+    arrive(1, s3_1)
+    produce(2)
     chip1 = chip_sum(1)
     out_half(0, 0, chip1[0], to_x)
     own[1, 64:128] = chip1[1]
-    arrive(1, s3_1)
-    produce(2)
     produce(3)
     chip2 = chip_sum(2)
     out_half(1, 1, chip2[1], to_y)

time: 76.8 us -> 76.3 us (level)
  no operation moved by 1% of the time
where the time goes in v6:
time: 76.3 us; the launch traced here: 76.1 us
  Pallas kernels  74.4 us (98%)
  local copies, waits for them, and re-layouts  1.67 us (2%)
    pallas_call x1, Pallas kernels, body(): pl.pallas_call(kernel, out_shape=jax.ShapeDtypeStruct((1, 128, 1024), BF1...  74.4 us
    unnamed x1, local copies, waits for them, and re-layouts  1.67 us

profile of v6, /device:TPU:1, one launch (start us, length us, event | category | flops | bytes accessed | tf_op | source)
XLA Modules:
  0.0 76.1 jit_solution(10309486684572237973)
XLA Ops:
  0.0 74.4 %shard_map.154 = bf16[1,128,1024]{2,1,0:T(8,128)(2,1)} custom-call(bf16[1,256,512]{2,1,0:T(8,128)(2,1)} %tok.1, bf16[16,1024]{1,0:T(8,128)(2,1)} %w_inner.1, bf16[16,1024]{1,0:T(8,128)(2,1)} %w_gate.1, bf16[16,256]{1,0:T(8,128)(2,1)} %w_write.1, bf16[16,256]{1,0:T(8,128)(2,1)} %w_read.1, bf16[16,512]{1,0:T(8,128)(2,1)} %w_pool.1, ...), custom_call_target="tpu_custom_call" | custom-call | tf_op jit(solution)/shard_map/pallas_call | solution.py:703
  74.4 1.7 %copy.18 = bf16[1,128,1024]{2,1,0:T(8,128)(2,1)} copy(bf16[1,128,1024]{2,1,0:T(8,128)(2,1)} %shard_map.154) | data formatting | bytes 524288
